TPU v7x, 512 devices: a whole 4x8x8 slice. The times are simulated.
512 devices in a mesh: sp: 64 (over z, y), fs: 4 (over x), tp: 2 (over core).
Axes of the slice: x: 4, y: 8, z: 8, core: 2. Of those that a mesh axis runs over, the one named last changes fastest.
Arguments:
- tokens: bfloat16 [4, 32768, 2048], P('fs', ('sp', 'tp')), may hold values from -6 to 6
- norm_gain: float32 [2048], replicated, may hold values from 0.1 to 1.9
- query_weight: bfloat16 [2048, 1024], P('sp', 'tp'), may hold values from -20 to 20
- key_matrix: bfloat16 [2048, 256], P('sp', 'tp'), may hold values from -0.125 to 0.125
- value_matrix: bfloat16 [2048, 256], P('sp', 'tp'), may hold values from -0.125 to 0.125
- pool_in_weight: bfloat16 [2048, 1024], P('sp', 'tp'), may hold values from -0.125 to 0.125
- head_sink_logit: float32 [16], replicated, may hold values from 2 to 6
- pool_mix: bfloat16 [4, 256, 256], replicated, may hold values from -0.375 to 0.375
- pool_gain: float32 [1024], replicated, may hold values from 0.1 to 1.9
- attn_out_weight: bfloat16 [1024, 2048], P('tp', 'sp'), may hold values from -1 to 1
- pool_out_weight: bfloat16 [1024, 2048], P('tp', 'sp'), may hold values from -0.125 to 0.125
Outputs:
- mixed: bfloat16 [4, 32768, 2048], P('fs', ('sp', 'tp'))
- row_log_weight_sum: float32 [4, 16, 32768], P('fs', 'tp', 'sp')
All inputs are finite; a program needn't handle non-finite values.
Results may differ from a plain program's by a relative error of at most 0.0095.
The roundings to bfloat16 on the way count: a program that leaves them out, or rounds other values in their place, can miss the bound.
Values may be sent and summed in bfloat16 or wider, within the bound.
A program may use at most 64 MiB of HBM per device.

v0:
```python
import jax
import jax.numpy as jnp
from jax import lax
from jax.sharding import PartitionSpec as P

HEAD_SIZE = 64
WINDOW = 128
POOL_CH = 256


EPSILON = 1e-06
POOL_SPANS = (2, 4, 8, 16)


def side_by_side(arrays, axis, dim, along):
    both = jnp.concatenate(arrays, axis=along)
    whole, at, outs = (lax.all_gather(both, axis, axis=dim, tiled=True), 0, [])
    for a in arrays:
        outs.append(lax.slice_in_dim(whole, at, at + a.shape[along], axis=along))
        at += a.shape[along]
    return tuple(outs)


def copy_for_each(shard, axis):
    size = lax.axis_size(axis)
    return lax.all_to_all(
        jnp.broadcast_to(shard[None], (size, *shard.shape)), axis, 0, 0, tiled=True
    )


def joined_along(blocks, dim):
    blocks = jnp.moveaxis(blocks, 0, dim)
    shape = blocks.shape
    return blocks.reshape(*shape[:dim], shape[dim] * shape[dim + 1], *shape[dim + 2 :])


def collect(shard, axis, dim):
    blocks = copy_for_each(shard, axis)
    return joined_along(blocks, dim)


def passed_along(shard, axis, by):
    size = lax.axis_size(axis)
    pairs = [(i, i + by) for i in range(size) if 0 <= i + by < size]
    return lax.ppermute(shard, axis, pairs)


def rows_first(arrays, axis, dims):
    turned = [jnp.moveaxis(a, dim, 0) for a, dim in zip(arrays, dims)]
    both = jnp.concatenate([t.reshape(len(t), -1) for t in turned], axis=1)
    whole, at, outs = (lax.all_gather(both, axis, axis=0, tiled=True), 0, [])
    for t, dim in zip(turned, dims):
        share = whole[:, at : at + t[0].size].reshape(-1, *t.shape[1:])
        outs.append(jnp.moveaxis(share, 0, dim))
        at += t[0].size
    return tuple(outs)


def in_blocks(shard, dim, size):
    shape = shard.shape
    blocks = shard.reshape(*shape[:dim], size, shape[dim] // size, *shape[dim + 1 :])
    return jnp.moveaxis(blocks, dim, 0)


def sum_at_owner(shard, axis, dim):
    blocks = in_blocks(shard, dim, lax.axis_size(axis))
    arrived = lax.all_to_all(blocks, axis, split_axis=0, concat_axis=0, tiled=True)
    return arrived.sum(axis=0)


def windowed_attend(
    query_rows, key_rows, value_rows, key_tail, value_tail, sinks, kv_heads, group, first_pos
):
    rows = query_rows.shape[0]
    blocks = rows // WINDOW
    width = key_rows.shape[1]
    ext_keys = jnp.concatenate([key_tail, key_rows], 0)
    ext_values = jnp.concatenate([value_tail, value_rows], 0)

    def banded(table):
        return jnp.concatenate(
            [
                table[:rows].reshape(blocks, WINDOW, width),
                table[WINDOW:].reshape(blocks, WINDOW, width),
            ],
            axis=1,
        )

    band_keys = banded(ext_keys).reshape(blocks, 2 * WINDOW, kv_heads, HEAD_SIZE)
    band_values = banded(ext_values).reshape(blocks, 2 * WINDOW, kv_heads, HEAD_SIZE)
    query_blocks = query_rows.reshape(blocks, WINDOW, kv_heads, group, HEAD_SIZE)
    scores = jnp.einsum(
        "bqkgd,bskd->bkgqs", query_blocks, band_keys, preferred_element_type=jnp.float32
    ) * HEAD_SIZE ** (-0.5)
    query_pos = first_pos + jnp.arange(rows).reshape(blocks, WINDOW, 1)
    key_pos = (
        first_pos
        - WINDOW
        + jnp.arange(blocks).reshape(blocks, 1, 1) * WINDOW
        + jnp.arange(2 * WINDOW).reshape(1, 1, 2 * WINDOW)
    )
    offset = query_pos - key_pos
    allowed = (offset >= 0) & (offset < WINDOW) & (key_pos >= 0)
    scores = jnp.where(allowed[:, None, None], scores, -jnp.inf)
    sink_grid = sinks.reshape(1, kv_heads, group, 1, 1)
    top = jnp.maximum(jnp.max(scores, axis=-1, keepdims=True), sink_grid)
    weights = jnp.exp(scores - top)
    total = jnp.sum(weights, axis=-1, keepdims=True) + jnp.exp(sink_grid - top)
    probs = (weights / total).astype(jnp.bfloat16)
    mixed = jnp.einsum(
        "bkgqs,bskd->bqkgd", probs, band_values, preferred_element_type=jnp.float32
    ).astype(jnp.bfloat16)
    row_log_weight_sum = (top + jnp.log(total))[..., 0]
    return (
        mixed.reshape(rows, kv_heads * group * HEAD_SIZE),
        row_log_weight_sum.transpose(1, 2, 0, 3).reshape(kv_heads * group, rows),
    )


def pool_branch(pool_rows, pool_tail, mixing, scales, group_start, first_pos):
    rows = pool_rows.shape[0]
    columns = pool_rows.shape[1]
    pool_reach = max(POOL_SPANS)
    extended = jnp.concatenate([pool_tail, pool_rows], 0).astype(jnp.float32)
    group_index = group_start + jnp.arange(columns) // POOL_CH
    span_table = jnp.array(POOL_SPANS, jnp.int32)
    matches = group_index[:, None] == jnp.arange(len(POOL_SPANS))[None, :]
    span_of_col = jnp.sum(jnp.where(matches, span_table[None, :], 0), axis=1)
    trailing = jnp.zeros((rows, columns), jnp.float32)
    for lag in range(pool_reach):
        trailing = trailing + jnp.where(
            lag < span_of_col[None, :], extended[pool_reach - lag : pool_reach - lag + rows], 0.0
        )
    position = first_pos + jnp.arange(rows)
    count = jnp.minimum(position[:, None] + 1, span_of_col[None, :]).astype(jnp.float32)
    centred = (trailing / count - extended[pool_reach:]).astype(jnp.bfloat16)
    grouped = centred.reshape(rows, columns // POOL_CH, POOL_CH)
    product = jnp.einsum(
        "rgc,gcd->rgd", grouped, mixing, preferred_element_type=jnp.float32
    ).reshape(rows, columns)
    return (product * scales).astype(jnp.bfloat16)


def local(
    tokens,
    norm_gain,
    query_weight,
    key_matrix,
    value_matrix,
    pool_in_weight,
    head_sink_logit,
    pool_mix,
    pool_gain,
    attn_out_weight,
    pool_out_weight,
):
    tp_index = lax.axis_index("tp")
    sp_index = lax.axis_index("sp")
    q_cols = query_weight.shape[1]
    kv_cols = key_matrix.shape[1]
    pool_cols = pool_in_weight.shape[1]
    q_heads = q_cols // HEAD_SIZE
    kv_heads = kv_cols // HEAD_SIZE
    groups_dev = pool_cols // POOL_CH
    full_query, full_key, full_value, full_pool = side_by_side(
        (query_weight, key_matrix, value_matrix, pool_in_weight), "sp", 0, 1
    )
    values_f = collect(tokens[0], "tp", 0).astype(jnp.float32)
    scale = lax.rsqrt(jnp.mean(values_f * values_f, axis=-1, keepdims=True) + EPSILON)
    normed = (values_f * scale * norm_gain).astype(jnp.bfloat16)
    outputs = [
        jnp.dot(normed, weight, preferred_element_type=jnp.float32).astype(jnp.bfloat16)
        for weight in (full_query, full_key, full_value, full_pool)
    ]
    projected = jnp.concatenate(outputs, axis=1)
    rows = projected.shape[0]
    first_pos = sp_index * rows
    query_rows = projected[:, :q_cols]
    key_rows = projected[:, q_cols : q_cols + kv_cols]
    value_rows = projected[:, q_cols + kv_cols : q_cols + 2 * kv_cols]
    pool_rows = projected[:, q_cols + 2 * kv_cols :]
    pool_reach = max(POOL_SPANS)
    sinks = lax.dynamic_slice_in_dim(head_sink_logit, tp_index * q_heads, q_heads, 0)
    mixing = lax.dynamic_slice_in_dim(pool_mix, tp_index * groups_dev, groups_dev, 0)
    scales = lax.dynamic_slice_in_dim(pool_gain, tp_index * pool_cols, pool_cols, 0)
    key_tail, value_tail, pool_tail = passed_along(
        (key_rows[rows - WINDOW :], value_rows[rows - WINDOW :], pool_rows[rows - pool_reach :]),
        "sp",
        1,
    )
    attn_part, log_part = windowed_attend(
        query_rows,
        key_rows,
        value_rows,
        key_tail,
        value_tail,
        sinks,
        kv_heads,
        q_heads // kv_heads,
        first_pos,
    )
    pool_part = pool_branch(pool_rows, pool_tail, mixing, scales, tp_index * groups_dev, first_pos)
    half_attn, half_pool = rows_first((attn_out_weight, pool_out_weight), "sp", (1, 1))
    result = sum_at_owner(
        jnp.dot(attn_part, half_attn, preferred_element_type=jnp.float32)
        + jnp.dot(pool_part, half_pool, preferred_element_type=jnp.float32),
        "tp",
        0,
    ).astype(jnp.bfloat16)
    return (result[None], log_part[None])


def solution(mesh):
    in_specs = (
        P("fs", ("sp", "tp"), None),
        P(),
        P("sp", "tp"),
        P("sp", "tp"),
        P("sp", "tp"),
        P("sp", "tp"),
        P(),
        P(),
        P(),
        P("tp", "sp"),
        P("tp", "sp"),
    )
    out_specs = (P("fs", ("sp", "tp"), None), P("fs", "tp", "sp"))
    return jax.shard_map(local, mesh=mesh, in_specs=in_specs, out_specs=out_specs, check_vma=False)
```

profile of v0, /device:TPU:1, one launch (start us, length us, event | category | flops | bytes accessed | tf_op | source)
XLA Modules:
  0.0 215.0 jit_solution(15751147720776613195)
XLA Ops:
  7.2 1.5 pad_maximum_fusion.2
  8.8 1.4 pad_maximum_fusion.3
  10.3 2.8 %broadcast_in_dim.162 = bf16[2,256,2048]{2,1,0:T(8,128)(2,1)} broadcast(bf16[256,2048]{1,0:T(8,128)(2,1)} %bitcast.82), dimensions={1,2} | broadcast | bytes 3145728 | tf_op jit(solution)/shard_map/broadcast_in_dim | solution.py:27
  13.1 10.6 %all-to-all-start = ((bf16[2,256,2048]{2,1,0:T(8,128)(2,1)}), bf16[2,256,2048]{2,1,0:T(8,128)(2,1)S(1)}, u32[]{:S(2)}, u32[]{:S(2)}) async-start(bf16[2,256,2048]{2,1,0:T(8,128)(2,1)} %broadcast_in_dim.162), calls=%async_computation | async-start | bytes 4194304 | tf_op jit(solution)/shard_map/all_to_all | solution.py:26
  23.7 0.1 dynamic_slice.9
  23.8 0.1 max.26
  23.8 2.3 %all-to-all-done = bf16[2,256,2048]{2,1,0:T(8,128)(2,1)S(1)} async-done(((bf16[2,256,2048]{2,1,0:T(8,128)(2,1)}), bf16[2,256,2048]{2,1,0:T(8,128)(2,1)S(1)}, u32[]{:S(2)}, u32[]{:S(2)}) %all-to-all-start) | async-done | bytes 2097184 | tf_op jit(solution)/shard_map/all_to_all | solution.py:26
  26.2 0.5 multiply_reduce_fusion
  26.7 0.1 dynamic_slice.11
  26.8 0.1 select_reduce_fusion
  26.9 0.1 broadcast_compare_fusion
  27.0 0.6 broadcast_compare_fusion.15
  27.7 0.3 fusion.49
  28.0 1.9 fusion.1
  29.9 71.3 %all-gather.3.cloned.1.call-done = bf16[2048,1280]{1,0:T(8,128)(2,1)} async-done(((bf16[32,1280]{1,0:T(8,128)(2,1)}), bf16[2048,1280]{1,0:T(8,128)(2,1)}) %all-gather.3.cloned.1.call-update) | async-done | bytes 5242896 | tf_op jit(solution)/shard_map/all_gather | solution.py:17
  101.3 2.4 %convolution_convert_fusion = bf16[512,128]{1,0:T(8,128)(2,1)S(1)} fusion(bf16[512,2048]{1,0:T(8,128)(2,1)} %fusion.1, bf16[2048,1280]{1,0:T(8,128)(2,1)} %all-gather.3.cloned.1.call-done), kind=kOutput, calls=%fused_computation.22 | convolution fusion | flops 268500992 | bytes 2752512 | tf_op jit(solution)/shard_map/dot_general | solution.py:172
  103.7 0.1 reshape.258
  103.8 2.9 %collective-permute-start.1 = (bf16[128,128]{1,0:T(8,128)(2,1)S(1)}, bf16[128,128]{1,0:T(8,128)(2,1)S(1)}, u32[]{:S(2)}, u32[]{:S(2)}) collective-permute-start(bf16[128,128]{1,0:T(8,128)(2,1)S(1)} %slice.112), channel_id=1, source_target_pairs={{0,8},{8,16},{16,24},{24,32},{32,40},{40,48},{48,56},{56,64},{64,7... | collective-permute-start | bytes 98312 | tf_op jit(solution)/shard_map/ppermute | solution.py:45
  106.7 2.4 %convolution_convert_fusion.1 = bf16[512,128]{1,0:T(8,128)(2,1)S(1)} fusion(bf16[512,2048]{1,0:T(8,128)(2,1)} %fusion.1, bf16[2048,1280]{1,0:T(8,128)(2,1)} %all-gather.3.cloned.1.call-done), kind=kOutput, calls=%fused_computation.23 | convolution fusion | flops 268500992 | bytes 2752512 | tf_op jit(solution)/shard_map/dot_general | solution.py:172
  109.1 3.2 %collective-permute-start = (bf16[128,128]{1,0:T(8,128)(2,1)S(1)}, bf16[128,128]{1,0:T(8,128)(2,1)S(1)}, u32[]{:S(2)}, u32[]{:S(2)}) collective-permute-start(bf16[128,128]{1,0:T(8,128)(2,1)S(1)} %slice.110), channel_id=1, source_target_pairs={{0,8},{8,16},{16,24},{24,32},{32,40},{40,48},{48,56},{56,64},{64,7... | collective-permute-start | bytes 98312 | tf_op jit(solution)/shard_map/ppermute | solution.py:45
  112.4 2.8 %fusion.15 = bf16[512,512]{1,0:T(8,128)(2,1)S(1)} fusion(bf16[512,2048]{1,0:T(8,128)(2,1)S(1)} %copy-done.2, bf16[2048,1280]{1,0:T(8,128)(2,1)} %all-gather.3.cloned.1.call-done), kind=kOutput, calls=%fused_computation.19 | convolution fusion | flops 1074003968 | bytes 4718592 | tf_op jit(solution)/shard_map/dot_general | solution.py:172
  115.2 0.7 slice.116
  115.9 3.5 %collective-permute-start.2 = (bf16[16,512]{1,0:T(8,128)(2,1)}, bf16[16,512]{1,0:T(8,128)(2,1)}, u32[]{:S(2)}, u32[]{:S(2)}) collective-permute-start(bf16[16,512]{1,0:T(8,128)(2,1)} %slice.116), channel_id=1, source_target_pairs={{0,8},{8,16},{16,24},{24,32},{32,40},{40,48},{48,56},{56,64},{64,7... | collective-permute-start | bytes 49160 | tf_op jit(solution)/shard_map/ppermute | solution.py:45
  119.4 3.7 %fusion.12 = bf16[512,512]{1,0:T(8,128)(2,1)} fusion(bf16[512,2048]{1,0:T(8,128)(2,1)S(1)} %copy-done.2, bf16[2048,1280]{1,0:T(8,128)(2,1)} %all-gather.3.cloned.1.call-done), kind=kOutput, calls=%fused_computation.18 | convolution fusion | flops 1074003968 | bytes 4718592 | tf_op jit(solution)/shard_map/dot_general | solution.py:172
  123.0 0.1 reshape.256
  123.2 0.1 copy.41
  123.3 0.1 copy.45
  123.5 2.2 %reshape.259 = bf16[4,128,2,4,64]{4,3,2,1,0:T(4,128)(2,1)S(1)} reshape(bf16[512,512]{1,0:T(8,128)(2,1)} %fusion.12) | data formatting | bytes 1048576 | tf_op jit(solution)/shard_map/reshape | solution.py:91
  125.7 1.2 maximum_convert_fusion
  126.9 3.8 %fusion.40 = bf16[512,512]{1,0:T(8,128)(2,1)S(1)} fusion(f32[528,512]{1,0:T(8,128)S(1)} %maximum_convert_fusion, s32[512]{0:T(512)S(1)} %select_reduce_fusion, s32[512]{0:T(512)S(1)} %add_add_fusion, pred[512]{0:T(512)(128)(4,1)} %get-tuple-element.3, pred[512]{0:T(512)(128)(4,1)} %get-tuple-element.4, pred[512]{0:T(512)(128)(4,1)} %get-tuple-element.5, ...), kind=kLoop, calls=%fused_computation.61 | loop fusion | flops 9437184 | bytes 17313792 | tf_op jit(solution)/shard_map/convert_element_type | solution.py:136
  130.7 0.4 fusion.43
  131.1 0.1 fusion.37
  131.2 0.1 reshape.255
  131.4 0.1 copy.40
  131.5 0.1 reshape.257
  131.7 0.1 copy.44
  131.8 0.9 fusion.3
  132.7 0.1 broadcast_maximum_fusion
  132.8 1.0 fusion.2
  133.8 0.1 exponential_add_fusion
  133.9 1.2 fusion.19
  135.1 0.4 copy.49
  135.5 0.7 fusion.56
  136.2 51.1 %all-gather.5.cloned.1.call-done = bf16[2048,1024]{1,0:T(8,128)(2,1)} async-done(((bf16[32,1024]{1,0:T(8,128)(2,1)}), bf16[2048,1024]{1,0:T(8,128)(2,1)}) %all-gather.5.cloned.1.call-update) | async-done | bytes 4194320 | tf_op jit(solution)/shard_map/all_gather | solution.py:51
  187.3 3.0 %fusion.7 = f32[512,2048]{1,0:T(8,128)S(1)} fusion(bf16[2048,1024]{1,0:T(8,128)(2,1)} %all-gather.5.cloned.1.call-done, bf16[64,8,4,128]{3,2,1,0:T(4,128)(2,1)S(1)} %bitcast.80), kind=kOutput, calls=%fused_computation.13 | convolution fusion | flops 1073741824 | bytes 6815744 | tf_op jit(solution)/shard_map/dot_general | solution.py:205
  190.4 1.4 convolution_add_fusion
  191.8 12.6 %all_to_all.10 = f32[2,256,2048]{2,1,0:T(8,128)} all-to-all(f32[2,256,2048]{2,1,0:T(8,128)S(1)} %bitcast.79), channel_id=1, replica_groups=mesh['sp'=64,'fs'=4,'tp'=2] {'tp'}, dimensions={0} | all-to-all | bytes 8388608 | tf_op jit(solution)/shard_map/all_to_all | solution.py:67
  204.4 3.8 %reduce_sum.41 = bf16[256,2048]{1,0:T(8,128)(2,1)} reduce(f32[2,256,2048]{2,1,0:T(8,128)} %all_to_all.10, f32[]{:T(128)} %constant.32.clone.1), dimensions={0}, to_apply=%region_4.5 | reduce | flops 524288 | bytes 5242884 | tf_op jit(solution)/shard_map/reduce_sum | solution.py:68
  (34 shorter events, 0.3 us)
Async XLA Ops:
  7.2 123.5 %copy-start = (bf16[4,256,256]{2,1,0:T(8,128)(2,1)S(1)}, bf16[4,256,256]{2,1,0:T(8,128)(2,1)}, u32[]{:S(2)}) copy-start(bf16[4,256,256]{2,1,0:T(8,128)(2,1)} %param.19) | copy-start | bytes 1572868
  7.2 16.5 %copy-start.7 = (f32[16]{0:T(128)S(1)}, f32[16]{0:T(128)}, u32[]{:S(2)}) copy-start(f32[16]{0:T(128)} %param.18) | copy-start | bytes 196
  7.2 94.1 %all-gather.3.cloned.1.call-start = ((), (), s32[]{:S(2)}) async-start(), calls=%async_computation.2 | async-start | bytes 5324800 | tf_op jit(solution)/shard_map/all_gather | solution.py:17
  8.8 178.6 %all-gather.5.cloned.1.call-start = ((), (), s32[]{:S(2)}) async-start(), calls=%async_computation.3 | async-start | bytes 4259840 | tf_op jit(solution)/shard_map/all_gather | solution.py:51
  10.2 16.4 %copy-start.5 = (f32[1024]{0:T(1024)S(1)}, f32[1024]{0:T(1024)}, u32[]{:S(2)}) copy-start(f32[1024]{0:T(1024)} %param.20) | copy-start | bytes 12292
  10.3 16.6 %copy-start.6 = (s32[4]{0:T(128)S(1)}, s32[4]{0:T(128)}, u32[]{:S(2)}) copy-start(s32[4]{0:T(128)} %constant.90.clone) | copy-start | bytes 52
  10.3 17.8 %copy-start.4 = (f32[2048]{0:T(1024)S(1)}, f32[2048]{0:T(1024)}, u32[]{:S(2)}) copy-start(f32[2048]{0:T(1024)} %param.13) | copy-start | bytes 24580
  13.1 13.1 %all-to-all-start = ((bf16[2,256,2048]{2,1,0:T(8,128)(2,1)}), bf16[2,256,2048]{2,1,0:T(8,128)(2,1)S(1)}, u32[]{:S(2)}, u32[]{:S(2)}) async-start(bf16[2,256,2048]{2,1,0:T(8,128)(2,1)} %broadcast_in_dim.162), calls=%async_computation | async-start | bytes 4194304 | tf_op jit(solution)/shard_map/all_to_all | solution.py:26
  29.9 82.5 %copy-start.2 = (bf16[512,2048]{1,0:T(8,128)(2,1)S(1)}, bf16[512,2048]{1,0:T(8,128)(2,1)}, u32[]{:S(2)}) copy-start(bf16[512,2048]{1,0:T(8,128)(2,1)} %fusion.1) | copy-start | bytes 6291460
  103.8 27.7 %collective-permute-start.1 = (bf16[128,128]{1,0:T(8,128)(2,1)S(1)}, bf16[128,128]{1,0:T(8,128)(2,1)S(1)}, u32[]{:S(2)}, u32[]{:S(2)}) collective-permute-start(bf16[128,128]{1,0:T(8,128)(2,1)S(1)} %slice.112), channel_id=1, source_target_pairs={{0,8},{8,16},{16,24},{24,32},{32,40},{40,48},{48,56},{56,64},{64,7... | collective-permute-start | bytes 98312 | tf_op jit(solution)/shard_map/ppermute | solution.py:45
  109.1 22.1 %collective-permute-start = (bf16[128,128]{1,0:T(8,128)(2,1)S(1)}, bf16[128,128]{1,0:T(8,128)(2,1)S(1)}, u32[]{:S(2)}, u32[]{:S(2)}) collective-permute-start(bf16[128,128]{1,0:T(8,128)(2,1)S(1)} %slice.110), channel_id=1, source_target_pairs={{0,8},{8,16},{16,24},{24,32},{32,40},{40,48},{48,56},{56,64},{64,7... | collective-permute-start | bytes 98312 | tf_op jit(solution)/shard_map/ppermute | solution.py:45
  115.2 4.1 %copy-start.3 = (bf16[512,512]{1,0:T(8,128)(2,1)}, bf16[512,512]{1,0:T(8,128)(2,1)S(1)}, u32[]{:S(2)}) copy-start(bf16[512,512]{1,0:T(8,128)(2,1)S(1)} %fusion.15) | copy-start | bytes 1572868
  115.9 9.8 %collective-permute-start.2 = (bf16[16,512]{1,0:T(8,128)(2,1)}, bf16[16,512]{1,0:T(8,128)(2,1)}, u32[]{:S(2)}, u32[]{:S(2)}) collective-permute-start(bf16[16,512]{1,0:T(8,128)(2,1)} %slice.116), channel_id=1, source_target_pairs={{0,8},{8,16},{16,24},{24,32},{32,40},{40,48},{48,56},{56,64},{64,7... | collective-permute-start | bytes 49160 | tf_op jit(solution)/shard_map/ppermute | solution.py:45
  187.3 3.1 %copy-start.1 = (bf16[2048,1024]{1,0:T(8,128)(2,1)S(1)}, bf16[2048,1024]{1,0:T(8,128)(2,1)}, u32[]{:S(2)}) copy-start(bf16[2048,1024]{1,0:T(8,128)(2,1)} %all-gather.5.cloned.1.call-done) | copy-start | bytes 12582916
Sparse Core Ops, SparseCore 0:
  11.6 89.6 all-gather.2
  104.3 82.9 all-gather.4
where the time goes:
time: 216 us; the launch traced here: 215 us
  waiting for transfers between devices  125 us (58%)
  starting transfers between devices  20.3 us (9%)
  matrix products  18.1 us (8%)
  other arithmetic  17.3 us (8%)
  between operations  14.4 us (7%)
  blocking collectives  12.6 us (6%)
  local copies, waits for them, and re-layouts  7.47 us (3%)
    all_gather x1, waiting for transfers between devices, side_by_side(): whole, at, outs = (lax.all_gather(both, axis, axis=dim, tiled=True), 0, [])  71.3 us
    all_gather x1, waiting for transfers between devices, rows_first(): whole, at, outs = (lax.all_gather(both, axis, axis=0, tiled=True), 0, [])  51.1 us
    all_to_all x1, blocking collectives, sum_at_owner(): lax.all_to_all(blocks, axis, split_axis=0, concat_axis=0, tiled=True)  12.6 us
    dot_general x4, matrix products, local(): jnp.dot(normed, weight, preferred_element_type=jnp.float32)  11.3 us
    all_to_all x1, starting transfers between devices, copy_for_each(): lax.all_to_all(jnp.broadcast_to(shard[None], (size, *shard.shape)), axis,...  10.6 us
    ppermute x3, starting transfers between devices, passed_along(): return lax.ppermute(shard, axis, pairs)  9.65 us
  transfers between devices with their start and end apart: 6, of which 3 were waited for; matrix products, arithmetic and copies ran while one was open for 15% of the time, Pallas kernels for 0%

commit v1 on v0

v1 whole, which is shorter than its diff:
```python
import jax
import jax.numpy as jnp
from jax import lax
from jax.experimental import pallas as pl
from jax.experimental.pallas import tpu as pltpu
from jax.sharding import PartitionSpec as P

RING = 8
SHARD = 32
HEAD = 64
WIN = 128
POOL_CH = 256
EPSILON = 1e-06
F32 = jnp.float32
BF16 = jnp.bfloat16
MESH = pl.DeviceIdType.MESH
SIGN = (1, -1)


def kernel(
    x_hbm, gain, wq, wk, wv, wp, sink, pmix, pgain, wa, wo,
    out, lse,
    zi, yi, zo, yo, xb, nb, accz, accy, qs, kx, vx, px, ma, mp, ob, rb,
    loc_sem, tok_sem, p1s, p1r, bks, bkr, hls, hlr, exs, exr,
):
    R = RING
    half = R // 2
    block = R * SHARD
    rows = xb.shape[0]
    own = rows // 2
    sp = lax.axis_index("sp")
    tp = lax.axis_index("tp")
    z, y = sp // R, sp % R
    mine = pl.multiple_of(tp * own, own)
    theirs = pl.multiple_of((1 - tp) * own, own)
    nq = wq.shape[1]

    def along_y(d):
        return {"sp": z * R + (y + d + R) % R}

    def along_z(d):
        return {"sp": ((z + d + R) % R) * R + y}

    streams = (
        (zi, z, y, along_y, along_z),
        (yi, y, z, along_z, along_y),
        (zo, z, y, along_y, along_z),
        (yo, y, z, along_z, along_y),
    )

    def first(k, d):
        buf, major, minor, peer, _ = streams[k]
        ref = buf.at[major, minor]
        return pltpu.make_async_remote_copy(
            src_ref=ref, dst_ref=ref, send_sem=p1s.at[k, d], recv_sem=p1r.at[k, d],
            device_id=peer(d), device_id_type=MESH,
        )

    def bulk(k, way, s, c):
        buf, major, _, _, peer = streams[k]
        sign = SIGN[way]
        ref = buf.at[(major - sign * (s - 1) + R) % R, pl.ds(c * half, half)]
        return pltpu.make_async_remote_copy(
            src_ref=ref, dst_ref=ref, send_sem=bks.at[k, way, s, c], recv_sem=bkr.at[k, way, s, c],
            device_id=peer(sign), device_id_type=MESH,
        )

    def is_sent(way, s, c):
        return s < half or (s == half and c == way)

    def forward(k, s, c):
        for way in (0, 1):
            if is_sent(way, s, c):
                bulk(k, way, s, c).wait_recv()
                if is_sent(way, s + 1, c):
                    bulk(k, way, s + 1, c).start()

    local = []

    def place(src, dst):
        copy = pltpu.make_async_copy(src, dst, loc_sem.at[len(local)])
        copy.start()
        local.append(copy)

    place(wq, zi.at[z, y, :, pl.ds(0, nq)])
    place(wk, zi.at[z, y, :, pl.ds(nq, wk.shape[1])])
    place(wp, yi.at[y, z, :, pl.ds(0, wp.shape[1])])
    place(wv, yi.at[y, z, :, pl.ds(wp.shape[1], wv.shape[1])])
    place(x_hbm, xb.at[pl.ds(mine, own)])
    place(wa, zo.at[z, y])
    place(wo, yo.at[y, z])

    barrier = pltpu.get_barrier_semaphore()
    peers = [{"tp": 1 - tp}]
    peers += [{"sp": (sp + d + R * R) % (R * R)} for d in (1, -1)]
    for d in range(1, R):
        peers += [along_y(d), along_z(d)]
    for peer in peers:
        pl.semaphore_signal(barrier, inc=1, device_id=peer, device_id_type=MESH)
    pl.semaphore_wait(barrier, len(peers))
    for copy in local:
        copy.wait()

    tokens = pltpu.make_async_remote_copy(
        src_ref=xb.at[pl.ds(mine, own)], dst_ref=xb.at[pl.ds(mine, own)],
        send_sem=tok_sem.at[0], recv_sem=tok_sem.at[1],
        device_id={"tp": 1 - tp}, device_id_type=MESH,
    )
    for d in (1, R - 1, 2, R - 2, 3, R - 3, half):
        if d < R:
            first(0, d).start()
            first(1, d).start()
    tokens.start()

    def norm(start):
        def body(i, carry):
            r = pl.multiple_of(start + i * 32, 32)
            v = xb[pl.ds(r, 32), :].astype(F32)
            scale = lax.rsqrt(jnp.mean(v * v, axis=1, keepdims=True) + EPSILON)
            n = (v * scale * gain[...]).astype(BF16)
            for j in range(R):
                nb[j, pl.ds(r, 32), :] = n[:, j * block : (j + 1) * block]
            return carry

        lax.fori_loop(0, own // 32, body, 0)

    norm(mine)
    px[0:WIN, :] = jnp.zeros((WIN, px.shape[1]), BF16)

    def zero(i, carry):
        r = pl.multiple_of(i * 32, 32)
        accz[pl.ds(r, 32), :] = jnp.zeros((32, accz.shape[1]), F32)
        accy[pl.ds(r, 32), :] = jnp.zeros((32, accy.shape[1]), F32)
        return carry

    lax.fori_loop(0, rows // 32, zero, 0)
    tokens.wait_recv()
    norm(theirs)

    def in_z(b):
        def body(m, carry):
            r = pl.multiple_of(m * own, own)
            w = zi[b].reshape(block, zi.shape[3])
            accz[pl.ds(r, own), :] += jnp.dot(nb[b, pl.ds(r, own), :], w, preferred_element_type=F32)
            return carry

        lax.fori_loop(0, 2, body, 0)

    def in_y(b):
        def body(m, carry):
            r = pl.multiple_of(m * own, own)
            w = yi[:, b].reshape(block, yi.shape[3])
            accy[pl.ds(r, own), :] += jnp.dot(nb[b, pl.ds(r, own), :], w, preferred_element_type=F32)
            return carry

        lax.fori_loop(0, 2, body, 0)

    def own_block(k):
        for d in range(1, R):
            first(k, d).wait_recv()
        for c in (0, 1):
            for way in (0, 1):
                if is_sent(way, 1, c):
                    bulk(k, way, 1, c).start()

    own_block(0)
    own_block(1)
    for d in range(1, R):
        first(2, d).start()
        first(3, d).start()
    in_z(z)
    for s in range(1, half):
        for c in (0, 1):
            forward(0, s, c)
            forward(1, s, c)
        in_z((z + s) % R)
        in_z((z - s + R) % R)
    own_block(2)
    own_block(3)
    for c in (0, 1):
        forward(0, half, c)
        forward(1, half, c)
    in_z((z + half) % R)

    def in_y_all(b, carry):
        in_y(b)
        return carry

    lax.fori_loop(0, R, in_y_all, 0)

    lane = lax.broadcasted_iota(jnp.int32, (32, 128), 1)

    def split(i, carry):
        r = pl.multiple_of(i * 32, 32)
        for p in range(nq // 128):
            t = accz[pl.ds(r, 32), p * 128 : (p + 1) * 128] * (HEAD ** (-0.5))
            turned = pltpu.roll(t, HEAD, 1)
            if p < nq // 256:
                even, odd, keep = t, turned, lane < HEAD
            else:
                even, odd, keep = turned, t, lane >= HEAD
            qs[2 * p, pl.ds(r, 32), :] = jnp.where(keep, even, 0.0).astype(BF16)
            qs[2 * p + 1, pl.ds(r, 32), :] = jnp.where(keep, odd, 0.0).astype(BF16)
        e = pl.multiple_of(WIN + i * 32, 32)
        kx[pl.ds(e, 32), :] = accz[pl.ds(r, 32), nq:].astype(BF16)
        vx[pl.ds(e, 32), :] = accy[pl.ds(r, 32), px.shape[1] :].astype(BF16)
        px[pl.ds(e, 32), :] = accy[pl.ds(r, 32), : px.shape[1]].astype(BF16)
        return carry

    lax.fori_loop(0, rows // 32, split, 0)

    def tail(i, ref, n):
        return pltpu.make_async_remote_copy(
            src_ref=ref.at[pl.ds(WIN + rows - n, n)], dst_ref=ref.at[pl.ds(WIN - n, n)],
            send_sem=hls.at[i], recv_sem=hlr.at[i],
            device_id={"sp": (sp + 1) % (R * R)}, device_id_type=MESH,
        )

    tails = (tail(0, kx, WIN), tail(1, vx, WIN), tail(2, px, 16))

    heads = qs.shape[0]
    group = heads // 2

    def attend(b):
        r = pl.multiple_of(b * WIN, WIN)
        keys = kx[pl.ds(r, 2 * WIN), :]
        values = vx[pl.ds(r, 2 * WIN), :]
        i = lax.broadcasted_iota(jnp.int32, (WIN, 2 * WIN), 0)
        j = lax.broadcasted_iota(jnp.int32, (WIN, 2 * WIN), 1)
        low = jnp.where((sp == 0) & (b == 0), WIN, 0)
        allowed = (j > i) & (j <= i + WIN) & (j >= low)
        lane = lax.broadcasted_iota(jnp.int32, (WIN, 128), 1)
        logs = jnp.zeros((WIN, 128), F32)
        outs = []
        for h in range(heads):
            score = lax.dot_general(
                qs[h, pl.ds(r, WIN), :], keys, (((1,), (1,)), ((), ())), preferred_element_type=F32
            )
            score = jnp.where(allowed, score, -jnp.inf)
            s = sink[tp * heads + h]
            top = jnp.maximum(jnp.max(score, axis=1, keepdims=True), s)
            weight = jnp.exp(score - top)
            total = jnp.sum(weight, axis=1, keepdims=True) + jnp.exp(s - top)
            probs = (weight * (1.0 / total)).astype(BF16)
            outs.append(jnp.dot(probs, values, preferred_element_type=F32))
            logs = jnp.where(lane == h, top + jnp.log(total), logs)
            if h % 2 == 1:
                even, odd = outs
                outs = []
                if h < group:
                    odd = pltpu.roll(odd, HEAD, 1)
                else:
                    even = pltpu.roll(even, HEAD, 1)
                p = h // 2
                ma[pl.ds(r, WIN), p * 128 : (p + 1) * 128] = jnp.where(lane < HEAD, even, odd).astype(BF16)
        lse[:, pl.ds(r, WIN)] = jnp.transpose(logs)[:heads, :]

    def pool(b):
        r = pl.multiple_of(b * WIN, WIN)
        i = lax.broadcasted_iota(jnp.int32, (WIN, 2 * WIN), 0)
        j = lax.broadcasted_iota(jnp.int32, (WIN, 2 * WIN), 1)
        low = jnp.where((sp == 0) & (b == 0), WIN, 0)
        lag = i + WIN - j
        pos = sp * rows + b * WIN + lax.broadcasted_iota(jnp.int32, (WIN, POOL_CH), 0)
        for g in range(px.shape[1] // POOL_CH):
            cols = slice(g * POOL_CH, (g + 1) * POOL_CH)
            span = jnp.where(tp == 0, 2 << g, 8 << g)
            band = jnp.where((lag >= 0) & (lag < span) & (j >= low), 1.0, 0.0).astype(BF16)
            ext = px[pl.ds(r, 2 * WIN), cols]
            trailing = jnp.dot(band, ext, preferred_element_type=F32)
            count = jnp.minimum(pos + 1, span).astype(F32)
            centred = (trailing / count - ext[WIN:].astype(F32)).astype(BF16)
            product = jnp.dot(centred, pmix[tp * 2 + g], preferred_element_type=F32)
            scales = pgain[pl.ds(tp * 2 + g, 1), :]
            mp[pl.ds(r, WIN), cols] = (product * scales).astype(BF16)

    def out_z(n):
        def body(m, carry):
            r = pl.multiple_of(m * own, own)
            w = zo[n].reshape(block, zo.shape[3])
            ob[n, pl.ds(r, own), :] = lax.dot_general(
                ma[pl.ds(r, own), :], w, (((1,), (1,)), ((), ())), preferred_element_type=F32
            )
            return carry

        lax.fori_loop(0, 2, body, 0)

    for t in tails:
        t.start()
    attend(1)
    forward(2, 1, 0)
    forward(3, 1, 0)
    attend(2)
    forward(2, 1, 1)
    forward(3, 1, 1)
    attend(3)
    forward(2, 2, 0)
    forward(3, 2, 0)
    for t in tails:
        t.wait_recv()
    attend(0)
    forward(2, 2, 1)
    forward(3, 2, 1)

    def pool_all(b, carry):
        pool(b)
        return carry

    lax.fori_loop(0, rows // WIN, pool_all, 0)
    for s in range(3, half):
        for c in (0, 1):
            forward(2, s, c)
            forward(3, s, c)
    out_z(z)
    for s in range(1, half):
        out_z((z + s) % R)
        out_z((z - s + R) % R)
    for c in (0, 1):
        forward(2, half, c)
    out_z((z + half) % R)
    for c in (0, 1):
        forward(3, half, c)

    def exchange(n):
        return pltpu.make_async_remote_copy(
            src_ref=ob.at[n, pl.ds(theirs, own)], dst_ref=rb.at[n],
            send_sem=exs.at[n], recv_sem=exr.at[n],
            device_id={"tp": 1 - tp}, device_id_type=MESH,
        )

    def out_y(n, r):
        w = yo[:, n].reshape(block, yo.shape[3])
        ob[n, pl.ds(r, own), :] += lax.dot_general(
            mp[pl.ds(r, own), :], w, (((1,), (1,)), ((), ())), preferred_element_type=F32
        )

    def give(n, carry):
        out_y(n, theirs)
        exchange(n).start()
        return carry

    lax.fori_loop(0, R, give, 0)

    def keep(n, carry):
        out_y(n, mine)
        return carry

    lax.fori_loop(0, R, keep, 0)
    for n in range(R):
        exchange(n).wait_recv()
        out[:, n * block : (n + 1) * block] = (ob[n, pl.ds(mine, own), :] + rb[n]).astype(BF16)

    tokens.wait_send()
    for t in tails:
        t.wait_send()
    for n in range(R):
        exchange(n).wait_send()
    for k in range(4):
        for d in range(1, R):
            first(k, d).wait_send()
        for way in (0, 1):
            for s in range(1, half + 1):
                for c in (0, 1):
                    if is_sent(way, s, c):
                        bulk(k, way, s, c).wait_send()


def local(
    tokens, norm_gain, query_weight, key_matrix, value_matrix, pool_in_weight,
    head_sink_logit, pool_mix, pool_gain, attn_out_weight, pool_out_weight,
):
    R = RING
    own, width = tokens.shape[1:]
    rows = 2 * own
    block = R * SHARD
    nq = query_weight.shape[1]
    nk = key_matrix.shape[1]
    npool = pool_in_weight.shape[1]
    heads = nq // HEAD
    groups = pool_mix.shape[0]
    vmem = pl.BlockSpec(memory_space=pltpu.VMEM)
    smem = pl.BlockSpec(memory_space=pltpu.SMEM)
    anywhere = pl.BlockSpec(memory_space=pl.ANY)
    dma = pltpu.SemaphoreType.DMA
    result, logs = pl.pallas_call(
        kernel,
        name="mixer",
        out_shape=(
            jax.ShapeDtypeStruct((own, width), BF16),
            jax.ShapeDtypeStruct((heads, rows), F32),
        ),
        in_specs=[anywhere, vmem, anywhere, anywhere, anywhere, anywhere, smem, vmem, vmem, anywhere, anywhere],
        out_specs=(vmem, vmem),
        scratch_shapes=[
            pltpu.VMEM((R, R, SHARD, nq + nk), BF16),
            pltpu.VMEM((R, R, SHARD, npool + nk), BF16),
            pltpu.VMEM((R, R, SHARD, attn_out_weight.shape[0]), BF16),
            pltpu.VMEM((R, R, SHARD, pool_out_weight.shape[0]), BF16),
            pltpu.VMEM((rows, width), BF16),
            pltpu.VMEM((R, rows, block), BF16),
            pltpu.VMEM((rows, nq + nk), F32),
            pltpu.VMEM((rows, npool + nk), F32),
            pltpu.VMEM((heads, rows, 128), BF16),
            pltpu.VMEM((WIN + rows, nk), BF16),
            pltpu.VMEM((WIN + rows, nk), BF16),
            pltpu.VMEM((WIN + rows, npool), BF16),
            pltpu.VMEM((rows, nq), BF16),
            pltpu.VMEM((rows, npool), BF16),
            pltpu.VMEM((R, rows, block), F32),
            pltpu.VMEM((R, own, block), F32),
            dma((7,)),
            dma((2,)),
            dma((4, R)),
            dma((4, R)),
            dma((4, 2, R // 2 + 1, 2)),
            dma((4, 2, R // 2 + 1, 2)),
            dma((3,)),
            dma((3,)),
            dma((R,)),
            dma((R,)),
        ],
        compiler_params=pltpu.CompilerParams(
            collective_id=0, has_side_effects=True, vmem_limit_bytes=56 * 1024 * 1024
        ),
    )(
        tokens[0],
        norm_gain[None],
        query_weight,
        key_matrix,
        value_matrix,
        pool_in_weight,
        head_sink_logit,
        pool_mix,
        pool_gain.reshape(groups, POOL_CH),
        attn_out_weight.T,
        pool_out_weight.T,
    )
    return (result[None], logs[None])


def solution(mesh):
    in_specs = (
        P("fs", ("sp", "tp"), None),
        P(),
        P("sp", "tp"),
        P("sp", "tp"),
        P("sp", "tp"),
        P("sp", "tp"),
        P(),
        P(),
        P(),
        P("tp", "sp"),
        P("tp", "sp"),
    )
    out_specs = (P("fs", ("sp", "tp"), None), P("fs", "tp", "sp"))
    return jax.shard_map(local, mesh=mesh, in_specs=in_specs, out_specs=out_specs, check_vma=False)
```

time: 216 us -> 98.2 us (0.45)
  waiting for transfers between devices: 125 us -> 0 us
  Pallas kernels: 0 us -> 93.1 us
  starting transfers between devices: 20.3 us -> 0 us
  matrix products: 18.1 us -> 0 us
  other arithmetic: 17.3 us -> 0 us
  between operations: 14.4 us -> 0.66 us
  blocking collectives: 12.6 us -> 0 us
  local copies, waits for them, and re-layouts: 7.47 us -> 4.2 us
    all_gather x2 -> x0, waiting for transfers between devices: 122 us -> none  [the longest x1 71.3 us: side_by_side(): whole, at, outs = (lax.all_gather(both, axis, axis=dim, tiled=True), 0, [])]
    pallas_call x0 -> x1, Pallas kernels: none -> 93.1 us  [local(): pl.pallas_call(kernel, name='mixer', out_shape=(jax.ShapeDtypeStruct((own...]
    dot_general x9 -> x0, matrix products: 18.1 us -> none  [the longest x4 11.3 us: local(): jnp.dot(normed, weight, preferred_element_type=jnp.float32)]
    all_to_all x1 -> x0, blocking collectives: 12.6 us -> none  [sum_at_owner(): lax.all_to_all(blocks, axis, split_axis=0, concat_axis=0, tiled=True)]
    all_to_all x1 -> x0, starting transfers between devices: 10.6 us -> none  [copy_for_each(): lax.all_to_all(jnp.broadcast_to(shard[None], (size, *shard.shape)), axis,...]
    ppermute x3 -> x0, starting transfers between devices: 9.65 us -> none  [passed_along(): return lax.ppermute(shard, axis, pairs)]
    convert_element_type x4 -> x0, other arithmetic: 7 us -> none  [the longest x1 3.83 us: pool_branch(): centred = (trailing / count - extended[pool_reach:]).astype(jnp.bfloat16)]
    reduce_sum x4 -> x0, other arithmetic: 5.33 us -> none  [the longest x1 3.78 us: sum_at_owner(): return arrived.sum(axis=0)]
  transfers between devices with their start and end apart: 6 -> 0, of which waited for: 3 -> 0; matrix products, arithmetic and copies ran while one was open for 15% -> 0% of each run, Pallas kernels for 0% -> 0%
where the time goes in v1:
time: 98.2 us; the launch traced here: 98 us
  Pallas kernels  93.1 us (95%)
  local copies, waits for them, and re-layouts  4.2 us (4%)
    pallas_call x1, Pallas kernels, local(): pl.pallas_call(kernel, name='mixer', out_shape=(jax.ShapeDtypeStruct((own...  93.1 us
    unnamed x6, local copies, waits for them, and re-layouts  3.6 us

profile of v1, /device:TPU:1, one launch (start us, length us, event | category | flops | bytes accessed | tf_op | source)
XLA Modules:
  0.0 98.0 jit_solution(18346046616358751535)
XLA Ops:
  0.6 0.0 copy-start.1
  0.6 0.7 copy-done.1
  1.3 0.6 reshape.7.pgain
  1.9 93.1 %mixer.1 = (bf16[256,2048]{1,0:T(8,128)(2,1)}, f32[8,512]{1,0:T(8,128)}) custom-call(bf16[256,2048]{1,0:T(8,128)(2,1)} %bitcast.6, f32[1,2048]{1,0:T(1,128)} %bitcast.11, bf16[32,512]{1,0:T(8,128)(2,1)} %wq.1, bf16[32,128]{1,0:T(8,128)(2,1)} %wk.1, bf16[32,128]{1,0:T(8,128)(2,1)} %wv.1, bf16[32,512]{1,0:T(8,128)(2,1)} %wp.1, f32[16]{0:T(128)} %sink.1, ...), custom_call_target="tpu_custom_call" | custom-call | tf_op jit(solution)/shard_map/mixer/pallas_call | solution.py:385
  95.1 0.0 copy-start
  95.1 2.3 %copy.15 = bf16[1,256,2048]{2,1,0:T(8,128)(2,1)} copy(bf16[1,256,2048]{2,1,0:T(8,128)(2,1)} %bitcast.7) | data formatting | bytes 2097152
  97.4 0.0 copy-done
  97.4 0.6 copy.16
Async XLA Ops:
  0.6 0.7 copy-start.1
  95.1 2.3 %copy-start = (f32[8,512]{1,0:T(8,128)S(1)}, f32[8,512]{1,0:T(8,128)}, u32[]{:S(2)}) copy-start(f32[8,512]{1,0:T(8,128)} %get-tuple-element.5) | copy-start | bytes 49156

commit v2 on v1

v2 whole, which is shorter than its diff:
```python
import jax
import jax.numpy as jnp
from jax import lax
from jax.experimental import pallas as pl
from jax.experimental.pallas import tpu as pltpu
from jax.sharding import PartitionSpec as P

RING = 8
CHUNKS = 4
SHARD = 32
HEAD = 64
WIN = 128
POOL_CH = 256
EPSILON = 1e-06
F32 = jnp.float32
BF16 = jnp.bfloat16
MESH = pl.DeviceIdType.MESH
SIGN = (1, -1)


def kernel(
    x_hbm, gain_hbm, wq, wk, wv, wp, sink, pmix_hbm, pgain_hbm, wa, wo,
    out, lse,
    zi, yi, zo, yo, xb, nb, accz, accy, qs, kx, vx, px, ma, mp, ob, rb, stage, gain, pmix, pgain,
    loc_sem, tok_sem, p1s, p1r, bks, bkr, xs, xr, hls, hlr, exs, exr, oss,
):
    R = RING
    NC = CHUNKS
    half = R // 2
    chunk = R // NC
    block = R * SHARD
    rows = xb.shape[0]
    own = rows // 2
    sp = lax.axis_index("sp")
    tp = lax.axis_index("tp")
    fs = lax.axis_index("fs")
    nfs = lax.axis_size("fs")
    par = fs % 2
    z, y = sp // R, sp % R
    mine = pl.multiple_of(tp * own, own)
    theirs = pl.multiple_of((1 - tp) * own, own)
    nq, nk, npool = wq.shape[1], wk.shape[1], wp.shape[1]
    heads = qs.shape[0]
    group = heads // 2
    scope = jax.named_scope

    def along_y(d):
        return {"sp": z * R + (y + d + R) % R}

    def along_z(d):
        return {"sp": ((z + d + R) % R) * R + y}

    streams = (
        (zi, z, y, along_y, along_z, nq // 2, 2 * nk),
        (yi, y, z, along_z, along_y, npool // 4, npool // 2),
        (zo, z, y, along_y, along_z, nq // 4, nq // 2),
        (yo, y, z, along_z, along_y, npool // 4, npool // 2),
    )

    def ring_cols(k):
        side, middle = streams[k][5:]
        return pl.ds(pl.multiple_of(par * side, 128), side + middle)

    def send(ref, send_sem, recv_sem, peer):
        return pltpu.make_async_remote_copy(
            src_ref=ref, dst_ref=ref, send_sem=send_sem, recv_sem=recv_sem,
            device_id=peer, device_id_type=MESH,
        )

    def first(k, d):
        buf, major, minor, peer = streams[k][:4]
        return send(buf.at[major, minor, :, ring_cols(k)], p1s.at[k, d], p1r.at[k, d], peer(d))

    def shard(k, way, s):
        buf, major, minor, peer = streams[k][:4]
        sign = SIGN[way]
        d = s if way == 0 else R - s
        ref = buf.at[major, (minor - sign * (s - 1) + R) % R, :, ring_cols(k)]
        return send(ref, p1s.at[k, d], p1r.at[k, d], peer(sign))

    def shard_is_sent(way, s):
        return s <= half if way == 0 else s < half

    def relay(k, s):
        for way in (0, 1):
            if s > 0 and shard_is_sent(way, s):
                shard(k, way, s).wait_recv()
            if shard_is_sent(way, s + 1):
                shard(k, way, s + 1).start()

    def bulk(k, way, s, c):
        buf, major, _, _, peer = streams[k][:5]
        sign = SIGN[way]
        ref = buf.at[(major - sign * (s - 1) + R) % R, pl.ds(c * chunk, chunk), :, ring_cols(k)]
        return send(ref, bks.at[k, way, s, c], bkr.at[k, way, s, c], peer(sign))

    def is_sent(way, s, c):
        return s < half or (s == half and (c < NC // 2) == (way == 0))

    def cross(k, j, c):
        buf, major = streams[k][:2]
        side, middle = streams[k][5:]
        cols = pl.ds(pl.multiple_of(par * (side + middle), 128), side)
        ref = buf.at[(major + j + R) % R, pl.ds(c * chunk, chunk), :, cols]
        step = 1 if c < NC // 2 else nfs - 1
        return send(ref, xs.at[k, j % R, c], xr.at[k, j % R, c], {"fs": (fs + step) % nfs})

    def crossed(k, j):
        for c in range(NC):
            cross(k, j, c).wait_recv()

    def own_block(k):
        for c in range(NC):
            for way in (0, 1):
                if is_sent(way, 1, c):
                    bulk(k, way, 1, c).start()
            cross(k, 0, c).start()

    def forward(k, s, c):
        for way in (0, 1):
            if is_sent(way, s, c):
                bulk(k, way, s, c).wait_recv()
                if is_sent(way, s + 1, c):
                    bulk(k, way, s + 1, c).start()
                cross(k, -SIGN[way] * s, c).start()

    local = []

    def place(src, dst):
        copy = pltpu.make_async_copy(src, dst, loc_sem.at[len(local)])
        copy.start()
        local.append(copy)

    side = pl.multiple_of(par * (nq // 2), 128)
    place(wq.at[:, pl.ds(side, nq // 2)], zi.at[z, y, :, pl.ds(pl.multiple_of(par * (nq // 2 + 2 * nk), 128), nq // 2)])
    place(wk, zi.at[z, y, :, pl.ds(nq // 2, nk)])
    place(wv, zi.at[z, y, :, pl.ds(nq // 2 + nk, nk)])
    place(wp.at[:, ring_cols(1)], yi.at[y, z, :, ring_cols(1)])
    place(wa.at[:, ring_cols(2)], zo.at[z, y, :, ring_cols(2)])
    place(wo.at[:, ring_cols(3)], yo.at[y, z, :, ring_cols(3)])
    place(x_hbm, xb.at[pl.ds(mine, own)])
    place(gain_hbm, gain)
    place(pmix_hbm.at[pl.ds(tp * pmix.shape[0], pmix.shape[0])], pmix)
    place(pgain_hbm.at[:, pl.ds(pl.multiple_of(tp * npool, 128), npool)], pgain)

    barrier = pltpu.get_barrier_semaphore()
    peers = [{"tp": 1 - tp}]
    peers += [{"sp": (sp + d + R * R) % (R * R)} for d in (1, -1)]
    peers += [{"fs": (fs + d) % nfs} for d in (1, nfs - 1)]
    for d in range(1, R):
        peers += [along_y(d), along_z(d)]
    for peer in peers:
        pl.semaphore_signal(barrier, inc=1, device_id=peer, device_id_type=MESH)
    with scope("barrier"):
        pl.semaphore_wait(barrier, len(peers))
        for copy in local:
            copy.wait()

    tokens = send(xb.at[pl.ds(mine, own)], tok_sem.at[0], tok_sem.at[1], {"tp": 1 - tp})
    for d in range(half, 0, -1):
        for e in sorted({d, R - d}):
            first(0, e).start()
            first(1, e).start()
    tokens.start()

    def norm(start):
        def body(i, carry):
            r = pl.multiple_of(start + i * 32, 32)
            v = xb[pl.ds(r, 32), :].astype(F32)
            scale = lax.rsqrt(jnp.mean(v * v, axis=1, keepdims=True) + EPSILON)
            n = (v * scale * gain[...]).astype(BF16)
            for j in range(R):
                nb[j, pl.ds(r, 32), :] = n[:, j * block : (j + 1) * block]
            return carry

        lax.fori_loop(0, own // 32, body, 0)

    def zero(i, carry):
        r = pl.multiple_of(i * 32, 32)
        accz[pl.ds(r, 32), :] = jnp.zeros((32, accz.shape[1]), F32)
        accy[pl.ds(r, 32), :] = jnp.zeros((32, accy.shape[1]), F32)
        return carry

    with scope("norm"):
        norm(mine)
        px[0:WIN, :] = jnp.zeros((WIN, npool), BF16)
        lax.fori_loop(0, rows // 32, zero, 0)
        tokens.wait_recv()
        norm(theirs)

    def in_z(j):
        b = (z + j + R) % R

        def body(m, carry):
            r = pl.multiple_of(m * own, own)
            w = zi[b].reshape(block, zi.shape[3])
            accz[pl.ds(r, own), :] += jnp.dot(nb[b, pl.ds(r, own), :], w, preferred_element_type=F32)
            return carry

        with scope("in_z"):
            crossed(0, j)
            lax.fori_loop(0, 2, body, 0)

    def in_y(first_b, n):
        def body(m, carry):
            b = first_b + m // 2
            r = pl.multiple_of((m % 2) * own, own)
            w = yi[:, b].reshape(block, yi.shape[3])
            accy[pl.ds(r, own), :] += jnp.dot(nb[b, pl.ds(r, own), :], w, preferred_element_type=F32)
            return carry

        with scope("in_y"):
            lax.fori_loop(0, 2 * n, body, 0)

    with scope("first"):
        for k in (0, 1):
            for d in range(1, R):
                first(k, d).wait_recv()
            own_block(k)
    relay(2, 0)
    relay(3, 0)

    steps = [(s, c) for s in range(1, half + 1) for c in range(NC)]
    relays = iter(range(1, half + 1))
    order = [0] + [j for s in range(1, half) for j in (s, -s)] + [half]
    ready = iter(order)
    for i, (s, c) in enumerate(steps):
        with scope("in_ring"):
            forward(0, s, c)
            forward(1, s, c)
        if i % 2 == 1:
            r = next(relays, None)
            if r is not None:
                with scope("relay"):
                    relay(2, r)
                    relay(3, r)
        if (s, c) == (half - 1, NC - 1):
            own_block(2)
            own_block(3)
        if s > 1 and c in (1, 2) and s <= half or (s, c) == (1, 2):
            in_z(next(ready))

    def split_z(i, carry):
        r = pl.multiple_of(i * 32, 32)
        lane = lax.broadcasted_iota(jnp.int32, (32, 128), 1)
        for p in range(heads // 2):
            at = p * 128 if p < heads // 4 else p * 128 + 2 * nk
            t = accz[pl.ds(r, 32), at : at + 128] * (HEAD ** (-0.5))
            turned = pltpu.roll(t, HEAD, 1)
            if p < heads // 4:
                even, odd, keep = t, turned, lane < HEAD
            else:
                even, odd, keep = turned, t, lane >= HEAD
            qs[2 * p, pl.ds(r, 32), :] = jnp.where(keep, even, 0.0).astype(BF16)
            qs[2 * p + 1, pl.ds(r, 32), :] = jnp.where(keep, odd, 0.0).astype(BF16)
        e = pl.multiple_of(WIN + i * 32, 32)
        kx[pl.ds(e, 32), :] = accz[pl.ds(r, 32), nq // 2 : nq // 2 + nk].astype(BF16)
        vx[pl.ds(e, 32), :] = accz[pl.ds(r, 32), nq // 2 + nk : nq // 2 + 2 * nk].astype(BF16)
        return carry

    def split_y(i, carry):
        r = pl.multiple_of(i * 32, 32)
        e = pl.multiple_of(WIN + i * 32, 32)
        px[pl.ds(e, 32), :] = accy[pl.ds(r, 32), :].astype(BF16)
        return carry

    def tail(i, ref, n):
        return pltpu.make_async_remote_copy(
            src_ref=ref.at[pl.ds(WIN + rows - n, n)], dst_ref=ref.at[pl.ds(WIN - n, n)],
            send_sem=hls.at[i], recv_sem=hlr.at[i],
            device_id={"sp": (sp + 1) % (R * R)}, device_id_type=MESH,
        )

    tails = (tail(0, kx, WIN), tail(1, vx, WIN), tail(2, px, 16))

    def attend(b):
        r = pl.multiple_of(b * WIN, WIN)
        keys = kx[pl.ds(r, 2 * WIN), :]
        values = vx[pl.ds(r, 2 * WIN), :]
        i = lax.broadcasted_iota(jnp.int32, (WIN, 2 * WIN), 0)
        j = lax.broadcasted_iota(jnp.int32, (WIN, 2 * WIN), 1)
        low = jnp.where((sp == 0) & (b == 0), WIN, 0)
        allowed = (j > i) & (j <= i + WIN) & (j >= low)
        lane = lax.broadcasted_iota(jnp.int32, (WIN, 128), 1)
        logs = jnp.zeros((WIN, 128), F32)
        outs = []
        for h in range(heads):
            score = lax.dot_general(
                qs[h, pl.ds(r, WIN), :], keys, (((1,), (1,)), ((), ())), preferred_element_type=F32
            )
            score = jnp.where(allowed, score, -jnp.inf)
            s = sink[tp * heads + h]
            top = jnp.maximum(jnp.max(score, axis=1, keepdims=True), s)
            weight = jnp.exp(score - top)
            total = jnp.sum(weight, axis=1, keepdims=True) + jnp.exp(s - top)
            probs = (weight * (1.0 / total)).astype(BF16)
            outs.append(jnp.dot(probs, values, preferred_element_type=F32))
            logs = jnp.where(lane == h, top + jnp.log(total), logs)
            if h % 2 == 1:
                even, odd = outs
                outs = []
                if h < group:
                    odd = pltpu.roll(odd, HEAD, 1)
                else:
                    even = pltpu.roll(even, HEAD, 1)
                p = h // 2
                ma[pl.ds(r, WIN), p * 128 : (p + 1) * 128] = jnp.where(lane < HEAD, even, odd).astype(BF16)
        lse[:, pl.ds(r, WIN)] = jnp.transpose(logs)[:heads, :]

    def attend_at(b):
        with scope("attend"):
            attend(b)

    def pool(b):
        r = pl.multiple_of(b * WIN, WIN)
        i = lax.broadcasted_iota(jnp.int32, (WIN, 2 * WIN), 0)
        j = lax.broadcasted_iota(jnp.int32, (WIN, 2 * WIN), 1)
        low = jnp.where((sp == 0) & (b == 0), WIN, 0)
        lag = i + WIN - j
        pos = sp * rows + b * WIN + lax.broadcasted_iota(jnp.int32, (WIN, POOL_CH), 0)
        for g in range(npool // POOL_CH):
            cols = slice(g * POOL_CH, (g + 1) * POOL_CH)
            span = jnp.where(tp == 0, 2 << g, 8 << g)
            band = jnp.where((lag >= 0) & (lag < span) & (j >= low), 1.0, 0.0).astype(BF16)
            ext = px[pl.ds(r, 2 * WIN), cols]
            trailing = jnp.dot(band, ext, preferred_element_type=F32)
            count = jnp.minimum(pos + 1, span).astype(F32)
            centred = (trailing / count - ext[WIN:].astype(F32)).astype(BF16)
            product = jnp.dot(centred, pmix[g], preferred_element_type=F32)
            mp[pl.ds(r, WIN), cols] = (product * pgain[:, cols]).astype(BF16)

    def pool_all(b, carry):
        pool(b)
        return carry

    def out_z(j):
        n = (z + j + R) % R

        def body(m, carry):
            r = pl.multiple_of(m * own, own)
            w = zo[n].reshape(block, zo.shape[3])
            ob[n, pl.ds(r, own), :] = lax.dot_general(
                ma[pl.ds(r, own), :], w, (((1,), (1,)), ((), ())), preferred_element_type=F32
            )
            return carry

        with scope("out_z"):
            crossed(2, j)
            lax.fori_loop(0, 2, body, 0)

    def split_all():
        with scope("split_z"):
            lax.fori_loop(0, rows // 32, split_z, 0)
            tails[0].start()
            tails[1].start()

    def in_y_ready():
        with scope("in_y_wait"):
            for j in order:
                crossed(1, j)

    def split_pool():
        with scope("split_y"):
            lax.fori_loop(0, rows // 32, split_y, 0)
            tails[2].start()

    def pool_now():
        with scope("tail_wait"):
            tails[0].wait_recv()
            tails[1].wait_recv()
            tails[2].wait_recv()
        with scope("pool"):
            lax.fori_loop(0, rows // WIN, pool_all, 0)

    pieces = [lambda j=j: in_z(j) for j in ready]
    pieces += [split_all, in_y_ready]
    pieces += [lambda b=b: in_y(b, 2) for b in range(0, R, 2)]
    pieces += [split_pool]
    pieces += [lambda b=b: attend_at(b) for b in range(1, rows // WIN)]
    pieces += [pool_now, lambda: attend_at(0)]
    late = [lambda j=j: out_z(j) for j in order]
    for i, (s, c) in enumerate(steps):
        if i < len(pieces):
            pieces[i]()
        with scope("out_ring"):
            forward(2, s, c)
            forward(3, s, c)
        if s == half and late:
            late.pop(0)()
    for piece in pieces[len(steps) :] + late:
        piece()

    def exchange(n):
        return pltpu.make_async_remote_copy(
            src_ref=ob.at[n, pl.ds(theirs, own)], dst_ref=rb.at[n],
            send_sem=exs.at[n], recv_sem=exr.at[n],
            device_id={"tp": 1 - tp}, device_id_type=MESH,
        )

    def result(n):
        cols = pl.ds(pl.multiple_of(n * block, 128), block)
        return pltpu.make_async_copy(stage.at[n], out.at[:, cols], oss.at[n])

    def out_y(n, r):
        w = yo[:, n].reshape(block, yo.shape[3])
        ob[n, pl.ds(r, own), :] += lax.dot_general(
            mp[pl.ds(r, own), :], w, (((1,), (1,)), ((), ())), preferred_element_type=F32
        )

    def give(n, carry):
        out_y(n, theirs)
        exchange(n).start()
        return carry

    def keep(n, carry):
        out_y(n, mine)
        exchange(n).wait_recv()
        stage[n] = (ob[n, pl.ds(mine, own), :] + rb[n]).astype(BF16)
        result(n).start()
        return carry

    with scope("out_y_wait"):
        for j in order:
            crossed(3, j)
    with scope("give"):
        lax.fori_loop(0, R, give, 0)
    with scope("keep"):
        lax.fori_loop(0, R, keep, 0)

    with scope("drain"):
        tokens.wait_send()
        for t in tails:
            t.wait_send()
        for k in range(4):
            for d in range(1, R):
                first(k, d).wait_send()
            for s, c in steps:
                for way in (0, 1):
                    if is_sent(way, s, c):
                        bulk(k, way, s, c).wait_send()
            for j in order:
                for c in range(NC):
                    cross(k, j, c).wait_send()
        for n in range(R):
            exchange(n).wait_send()
            result(n).wait()


def local(
    tokens, norm_gain, query_weight, key_matrix, value_matrix, pool_in_weight,
    head_sink_logit, pool_mix, pool_gain, attn_out_weight, pool_out_weight,
):
    R = RING
    own, width = tokens.shape[1:]
    rows = 2 * own
    block = R * SHARD
    nq = query_weight.shape[1]
    nk = key_matrix.shape[1]
    npool = pool_in_weight.shape[1]
    heads = nq // HEAD
    groups = pool_mix.shape[0]
    vmem = pl.BlockSpec(memory_space=pltpu.VMEM)
    smem = pl.BlockSpec(memory_space=pltpu.SMEM)
    anywhere = pl.BlockSpec(memory_space=pl.ANY)
    dma = pltpu.SemaphoreType.DMA
    result, logs = pl.pallas_call(
        kernel,
        name="mixer",
        out_shape=(
            jax.ShapeDtypeStruct((own, width), BF16),
            jax.ShapeDtypeStruct((heads, rows), F32),
        ),
        in_specs=[anywhere] * 6 + [smem] + [anywhere] * 4,
        out_specs=(anywhere, vmem),
        scratch_shapes=[
            pltpu.VMEM((R, R, SHARD, nq + 2 * nk), BF16),
            pltpu.VMEM((R, R, SHARD, npool), BF16),
            pltpu.VMEM((R, R, SHARD, attn_out_weight.shape[0]), BF16),
            pltpu.VMEM((R, R, SHARD, pool_out_weight.shape[0]), BF16),
            pltpu.VMEM((rows, width), BF16),
            pltpu.VMEM((R, rows, block), BF16),
            pltpu.VMEM((rows, nq + 2 * nk), F32),
            pltpu.VMEM((rows, npool), F32),
            pltpu.VMEM((heads, rows, 128), BF16),
            pltpu.VMEM((WIN + rows, nk), BF16),
            pltpu.VMEM((WIN + rows, nk), BF16),
            pltpu.VMEM((WIN + rows, npool), BF16),
            pltpu.VMEM((rows, nq), BF16),
            pltpu.VMEM((rows, npool), BF16),
            pltpu.VMEM((R, rows, block), F32),
            pltpu.VMEM((R, own, block), F32),
            pltpu.VMEM((R, own, block), BF16),
            pltpu.VMEM((1, width), F32),
            pltpu.VMEM((groups // 2, POOL_CH, POOL_CH), BF16),
            pltpu.VMEM((1, npool), F32),
            dma((10,)),
            dma((2,)),
            dma((4, R)),
            dma((4, R)),
            dma((4, 2, R // 2 + 1, CHUNKS)),
            dma((4, 2, R // 2 + 1, CHUNKS)),
            dma((4, R, CHUNKS)),
            dma((4, R, CHUNKS)),
            dma((3,)),
            dma((3,)),
            dma((R,)),
            dma((R,)),
            dma((R,)),
        ],
        compiler_params=pltpu.CompilerParams(
            collective_id=0, has_side_effects=True, vmem_limit_bytes=56 * 1024 * 1024
        ),
    )(
        tokens[0],
        norm_gain[None],
        query_weight,
        key_matrix,
        value_matrix,
        pool_in_weight,
        head_sink_logit,
        pool_mix,
        pool_gain[None],
        attn_out_weight.T,
        pool_out_weight.T,
    )
    return (result[None], logs[None])


def solution(mesh):
    in_specs = (
        P("fs", ("sp", "tp"), None),
        P(),
        P("sp", "tp"),
        P("sp", "tp"),
        P("sp", "tp"),
        P("sp", "tp"),
        P(),
        P(),
        P(),
        P("tp", "sp"),
        P("tp", "sp"),
    )
    out_specs = (P("fs", ("sp", "tp"), None), P("fs", "tp", "sp"))
    return jax.shard_map(local, mesh=mesh, in_specs=in_specs, out_specs=out_specs, check_vma=False)
```

time: 98.2 us -> 92.3 us (0.940)
  Pallas kernels: 93.1 us -> 88.6 us
  local copies, waits for them, and re-layouts: 4.2 us -> 2.92 us
    pallas_call x1, Pallas kernels: 93.1 us -> 88.6 us  [local(): pl.pallas_call(kernel, name='mixer', out_shape=(jax.ShapeDtypeStruct((own...]
    unnamed x6 -> x4, local copies, waits for them, and re-layouts: 3.6 us -> 2.92 us
where the time goes in v2:
time: 92.3 us; the launch traced here: 92.2 us
  Pallas kernels  88.6 us (96%)
  local copies, waits for them, and re-layouts  2.92 us (3%)
    pallas_call x1, Pallas kernels, local(): pl.pallas_call(kernel, name='mixer', out_shape=(jax.ShapeDtypeStruct((own...  88.6 us
    unnamed x4, local copies, waits for them, and re-layouts  2.92 us

profile of v2, /device:TPU:1, one launch (start us, length us, event | category | flops | bytes accessed | tf_op | source)
XLA Modules:
  0.0 92.2 jit_solution(18232718972623619582)
XLA Ops:
  0.6 88.6 %mixer.1 = (bf16[256,2048]{1,0:T(8,128)(2,1)}, f32[8,512]{1,0:T(8,128)}) custom-call(bf16[256,2048]{1,0:T(8,128)(2,1)} %bitcast.7, f32[1,2048]{1,0:T(1,128)} %bitcast.12, bf16[32,512]{1,0:T(8,128)(2,1)} %wq.1, bf16[32,128]{1,0:T(8,128)(2,1)} %wk.1, bf16[32,128]{1,0:T(8,128)(2,1)} %wv.1, bf16[32,512]{1,0:T(8,128)(2,1)} %wp.1, f32[16]{0:T(128)} %sink.1, ...), custom_call_target="tpu_custom_call" | custom-call | tf_op jit(solution)/shard_map/mixer/pallas_call | solution.py:466
  89.2 0.0 copy-start
  89.2 2.3 %copy.15 = bf16[1,256,2048]{2,1,0:T(8,128)(2,1)} copy(bf16[1,256,2048]{2,1,0:T(8,128)(2,1)} %bitcast.8) | data formatting | bytes 2097152
  91.6 0.0 copy-done
  91.6 0.6 copy.16
Async XLA Ops:
  89.2 2.3 %copy-start = (f32[8,512]{1,0:T(8,128)S(1)}, f32[8,512]{1,0:T(8,128)}, u32[]{:S(2)}) copy-start(f32[8,512]{1,0:T(8,128)} %get-tuple-element.5) | copy-start | bytes 49156

commit v3 on v2

v3 whole, which is shorter than its diff:
```python
import jax
import jax.numpy as jnp
from jax import lax
from jax.experimental import pallas as pl
from jax.experimental.pallas import tpu as pltpu
from jax.sharding import PartitionSpec as P

RING = 8
CHUNKS = 4
SHARD = 32
HEAD = 64
WIN = 128
POOL_CH = 256
EPSILON = 1e-06
F32 = jnp.float32
BF16 = jnp.bfloat16
MESH = pl.DeviceIdType.MESH
SIGN = (1, -1)


def kernel(
    x_hbm, gain_hbm, wq, wk, wv, wp, sink_hbm, pmix_hbm, pgain_hbm, wa, wo,
    out, lse,
    zi, yi, zo, yo, xb, nb, accz, accy, qs, kx, vx, px, ma, mp, ob, rb, sink, gain, pmix, pgain,
    loc_sem, tok_sem, sent, p1r, bkr, xr, hls, hlr, exs, exr,
):
    R = RING
    NC = CHUNKS
    half = R // 2
    chunk = R // NC
    block = R * SHARD
    rows = xb.shape[0]
    own = rows // 2
    sp = lax.axis_index("sp")
    tp = lax.axis_index("tp")
    fs = lax.axis_index("fs")
    nfs = lax.axis_size("fs")
    par = fs % 2
    z, y = sp // R, sp % R
    mine = pl.multiple_of(tp * own, own)
    theirs = pl.multiple_of((1 - tp) * own, own)
    nq, nk, npool = wq.shape[1], wk.shape[1], wp.shape[1]
    heads = nq // HEAD
    scope = jax.named_scope

    def along_y(d):
        return {"sp": z * R + (y + d + R) % R}

    def along_z(d):
        return {"sp": ((z + d + R) % R) * R + y}

    a, b = z + tp * (y - z), y + tp * (z - y)
    stride_a, stride_b = R - tp * (R - 1), 1 + tp * (R - 1)

    def along_a(d):
        return {"sp": (a + d + R) % R * stride_a + b * stride_b}

    def along_b(d):
        return {"sp": a * stride_a + (b + d + R) % R * stride_b}

    streams = (
        (zi, a, b, along_b, along_a, nq // 2, 2 * nk),
        (yi, b, a, along_a, along_b, npool // 4, npool // 2),
        (zo, z, y, along_y, along_z, nq // 4, nq // 2),
        (yo, y, z, along_z, along_y, npool // 4, npool // 2),
    )

    def ring_cols(k):
        side, middle = streams[k][5:]
        return pl.ds(pl.multiple_of(par * side, 128), side + middle)

    def send(ref, send_sem, recv_sem, peer):
        return pltpu.make_async_remote_copy(
            src_ref=ref, dst_ref=ref, send_sem=send_sem, recv_sem=recv_sem,
            device_id=peer, device_id_type=MESH,
        )

    def first(k, d):
        buf, major, minor, peer = streams[k][:4]
        return send(buf.at[major, minor, :, ring_cols(k)], sent.at[k, 2], p1r.at[k, d], peer(d))

    def second(k, d, hop):
        buf, major, minor, peer = streams[k][:4]
        ref = buf.at[major, (minor - d + R) % R, :, ring_cols(k)]
        return send(ref, sent.at[k, 2], p1r.at[k, (d + hop) % R], peer(hop))

    FURTHER = ((2, 1), (R - 2, -1), (2, 2))

    def piece_of(k, c):
        start = (streams[k][2] // chunk + c + (c // 2) * (5 - 2 * c)) % NC
        return pl.ds(start * chunk, chunk)

    def bulk(k, way, s, c):
        buf, major, _, _, peer = streams[k][:5]
        sign = SIGN[way]
        ref = buf.at[(major - sign * (s - 1) + R) % R, piece_of(k, c), :, ring_cols(k)]
        return send(ref, sent.at[k, 0], bkr.at[k, way, s, c], peer(sign))

    def is_sent(way, s, c):
        return s < half or (s == half and (c < NC // 2) == (way == 0))

    def side_cols(k, p):
        side, middle = streams[k][5:]
        return pl.ds(pl.multiple_of(p * (side + middle), 128), side)

    def cross(k, j, c):
        buf, major = streams[k][:2]
        ref = buf.at[(major + j + R) % R, piece_of(k, c), :, side_cols(k, par)]
        step = 1 + (nfs - 2) * (c // (NC // 2))
        return send(ref, sent.at[k, 1], xr.at[k, j % R], {"fs": (fs + step) % nfs})

    def crossed(k, j):
        buf, major = streams[k][:2]
        ref = buf.at[(major + j + R) % R, :, :, side_cols(k, 1 - par)]
        send(ref, sent.at[k, 1], xr.at[k, j % R], {"fs": (fs + 1) % nfs}).wait_recv()

    def own_piece(k, c):
        for way in (0, 1):
            bulk(k, way, 1, c).start()

    def forward(k, s, c):
        for way in (0, 1):
            if is_sent(way, s, c):
                bulk(k, way, s, c).wait_recv()
                if is_sent(way, s + 1, c):
                    bulk(k, way, s + 1, c).start()
                cross(k, -SIGN[way] * s, c).start()

    barrier = pltpu.get_barrier_semaphore()
    peers = [{"tp": 1 - tp}]
    peers += [{"sp": (sp + d + R * R) % (R * R)} for d in (1, -1)]
    peers += [{"fs": (fs + d) % nfs} for d in (1, nfs - 1)]
    for d in range(1, R):
        peers += [along_y(d), along_z(d)]
    for peer in peers:
        pl.semaphore_signal(barrier, inc=1, device_id=peer, device_id_type=MESH)

    local = []

    def place(src, dst):
        copy = pltpu.make_async_copy(src, dst, loc_sem.at[len(local)])
        copy.start()
        local.append(copy)

    side = pl.multiple_of(par * (nq // 2), 128)
    place(wq.at[:, pl.ds(side, nq // 2)], zi.at[a, b, :, pl.ds(pl.multiple_of(par * (nq // 2 + 2 * nk), 128), nq // 2)])
    place(wk, zi.at[a, b, :, pl.ds(nq // 2, nk)])
    place(wv, zi.at[a, b, :, pl.ds(nq // 2 + nk, nk)])
    place(wp.at[:, ring_cols(1)], yi.at[b, a, :, ring_cols(1)])
    place(wa.at[:, ring_cols(2)], zo.at[z, y, :, ring_cols(2)])
    place(wo.at[:, ring_cols(3)], yo.at[y, z, :, ring_cols(3)])
    place(x_hbm, xb.at[pl.ds(mine, own)])
    place(gain_hbm, gain)
    place(sink_hbm, sink)
    place(pmix_hbm.at[pl.ds(tp * pmix.shape[0], pmix.shape[0])], pmix)
    place(pgain_hbm.at[:, pl.ds(pl.multiple_of(tp * npool, 128), npool)], pgain)

    with scope("barrier"):
        pl.semaphore_wait(barrier, len(peers))
        for copy in local:
            copy.wait()

    tokens = send(xb.at[pl.ds(mine, own)], tok_sem.at[0], tok_sem.at[1], {"tp": 1 - tp})
    def norm(start):
        def body(i, carry):
            r = pl.multiple_of(start + i * 32, 32)
            v = xb[pl.ds(r, 32), :].astype(F32)
            scale = lax.rsqrt(jnp.mean(v * v, axis=1, keepdims=True) + EPSILON)
            n = v * scale * gain[...]
            for j in range(R):
                nb[tp, j, pl.ds(r, 32), :] = n[:, j * block : (j + 1) * block].astype(BF16)
            lane = lax.broadcasted_iota(jnp.int32, (32, 128), 1) // SHARD
            for j in range(R):
                for g in range(block // 128):
                    t = None
                    for q in range(128 // SHARD):
                        at = (g * (128 // SHARD) + q) * block + j * SHARD
                        a = n[:, at // 128 * 128 : at // 128 * 128 + 128]
                        turn = (q * SHARD - at % 128) % 128
                        a = pltpu.roll(a, turn, 1) if turn else a
                        t = a if t is None else jnp.where(lane == q, a, t)
                    nb[1 - tp, j, pl.ds(r, 32), g * 128 : (g + 1) * 128] = t.astype(BF16)
            return carry

        lax.fori_loop(0, own // 32, body, 0)

    def zero(i, carry):
        r = pl.multiple_of(i * 32, 32)
        accz[pl.ds(r, 32), :] = jnp.zeros((32, accz.shape[1]), F32)
        accy[pl.ds(r, 32), :] = jnp.zeros((32, accy.shape[1]), F32)
        return carry

    def in_z(j):
        n = (a + j + R) % R
        with scope("in_z"):
            crossed(0, j)
            accz[...] += jnp.dot(nb[0, n], zi[n].reshape(block, zi.shape[3]), preferred_element_type=F32)

    def in_y(j):
        n = (b + j + R) % R
        with scope("in_y"):
            crossed(1, j)
            accy[...] += jnp.dot(nb[1, n], yi[n].reshape(block, yi.shape[3]), preferred_element_type=F32)

    for d in (half, 3, R - 3, 2, R - 2, 1, R - 1):
        first(0, d).start()
        first(1, d).start()
    tokens.start()
    with scope("norm"):
        lax.fori_loop(0, rows // 32, zero, 0)
        norm(mine)
    for k in (2, 3):
        for d in (1, R - 1, 2, R - 2):
            first(k, d).start()
    with scope("norm"):
        px[0:WIN, :] = jnp.zeros((WIN, npool), BF16)
        tokens.wait_recv()
        norm(theirs)
    with scope("first"):
        for k in (0, 1):
            for d in range(1, R):
                first(k, d).wait_recv()
        for c in range(NC):
            for k in (0, 1):
                own_piece(k, c)
                cross(k, 0, c).start()

    order = [0] + [j for s in range(1, half) for j in (s, -s)] + [half]
    ready = [lambda j=j, f=f: f(j) for j in order for f in (in_z, in_y)]
    steps = [(s, c) for s in range(1, half) for c in range(NC)]
    steps += [(half, c) for c in (0, 2, 1, 3)]
    for i, (s, c) in enumerate(steps):
        with scope("in_ring"):
            forward(0, s, c)
            forward(1, s, c)
        if i == 1:
            with scope("second"):
                for k in (2, 3):
                    first(k, 2).wait_recv()
                    first(k, R - 2).wait_recv()
                    for d, hop in FURTHER:
                        second(k, d, hop).start()
        if i == 3 * NC - 1:
            with scope("own_out"):
                for k in (2, 3):
                    for d in range(1, R):
                        if d not in (2, R - 2):
                            first(k, d).wait_recv()
                    for n in range(NC):
                        own_piece(k, n)
        if i in (2, 3) or i > NC:
            ready.pop(0)()
    for k in (2, 3):
        for c in range(NC):
            cross(k, 0, c).start()

    def split_z(i, carry):
        r = pl.multiple_of(i * 32, 32)
        e = pl.multiple_of(WIN + i * 32, 32)
        for p in range(heads // 2):
            at = p * 128 if p < heads // 4 else p * 128 + 2 * nk
            q = accz[pl.ds(r, 32), at : at + 128] * (HEAD ** (-0.5))
            qs[pl.ds(r, 32), p * 128 : (p + 1) * 128] = q.astype(BF16)
        for ref, at in ((kx, nq // 2), (vx, nq // 2 + nk)):
            t = accz[pl.ds(r, 32), at : at + nk]
            ref[0, pl.ds(e, 32), :] = t.astype(BF16)
            ref[1, pl.ds(e, 32), :] = pltpu.roll(t, HEAD, 1).astype(BF16)
        return carry

    def split_y(i, carry):
        r = pl.multiple_of(i * 32, 32)
        e = pl.multiple_of(WIN + i * 32, 32)
        px[pl.ds(e, 32), :] = accy[pl.ds(r, 32), :].astype(BF16)
        return carry

    def tail(i, ref, n):
        src, dst = pl.ds(WIN + rows - n, n), pl.ds(WIN - n, n)
        return pltpu.make_async_remote_copy(
            src_ref=ref.at[src] if i == 2 else ref.at[:, src],
            dst_ref=ref.at[dst] if i == 2 else ref.at[:, dst],
            send_sem=hls.at[i], recv_sem=hlr.at[i],
            device_id={"sp": (sp + 1) % (R * R)}, device_id_type=MESH,
        )

    tails = (tail(0, kx, WIN), tail(1, vx, WIN), tail(2, px, 16))

    def attend(b):
        r = pl.multiple_of(b * WIN, WIN)
        i = lax.broadcasted_iota(jnp.int32, (WIN, WIN), 0)
        j = lax.broadcasted_iota(jnp.int32, (WIN, 128), 1)
        older = j > i
        missing = jnp.where((sp == 0) & (b == 0), -jnp.inf, 0.0)
        left = j < HEAD
        halves = (jnp.where(left, 1.0, 0.0).astype(BF16), jnp.where(left, 0.0, 1.0).astype(BF16))
        logs = jnp.zeros((WIN, 128), F32)
        for p in range(heads // 2):
            pair = qs[pl.ds(r, WIN), p * 128 : (p + 1) * 128]
            outs = []
            for odd in (0, 1):
                h = 2 * p + odd
                turned = odd ^ (h // (heads // 2))
                score = lax.dot_general(
                    pair * halves[odd], kx[turned, pl.ds(r, 2 * WIN), :], (((1,), (1,)), ((), ())),
                    preferred_element_type=F32,
                )
                score = jnp.where(older, score[:, :WIN] + missing, score[:, WIN:])
                s = sink[tp * heads + h]
                top = jnp.maximum(jnp.max(score, axis=1, keepdims=True), s)
                weight = jnp.exp(score - top)
                total = jnp.sum(weight, axis=1, keepdims=True) + jnp.exp(s - top)
                probs = weight * (1.0 / total)
                band = jnp.concatenate(
                    [jnp.where(older, probs, 0.0).astype(BF16), jnp.where(older, 0.0, probs).astype(BF16)], axis=1
                )
                outs.append(jnp.dot(band, vx[turned, pl.ds(r, 2 * WIN), :], preferred_element_type=F32))
                logs = jnp.where(j == h, top + jnp.log(total), logs)
            ma[pl.ds(r, WIN), p * 128 : (p + 1) * 128] = jnp.where(left, outs[0], outs[1]).astype(BF16)
        lse[:, pl.ds(r, WIN)] = jnp.transpose(logs)[:heads, :]

    def attend_at(b):
        with scope("attend"):
            attend(b)

    def pool(b):
        r = pl.multiple_of(b * WIN, WIN)
        i = lax.broadcasted_iota(jnp.int32, (WIN, 2 * WIN), 0)
        j = lax.broadcasted_iota(jnp.int32, (WIN, 2 * WIN), 1)
        low = jnp.where((sp == 0) & (b == 0), WIN, 0)
        lag = i + WIN - j
        pos = sp * rows + b * WIN + lax.broadcasted_iota(jnp.int32, (WIN, 1), 0)
        for g in range(npool // POOL_CH):
            cols = slice(g * POOL_CH, (g + 1) * POOL_CH)
            span = jnp.where(tp == 0, 2 << g, 8 << g)
            band = jnp.where((lag >= 0) & (lag < span) & (j >= low), 1.0, 0.0).astype(BF16)
            ext = px[pl.ds(r, 2 * WIN), cols]
            trailing = jnp.dot(band, ext, preferred_element_type=F32)
            count = jnp.minimum(pos + 1, span).astype(F32)
            centred = (trailing * (1.0 / count) - ext[WIN:].astype(F32)).astype(BF16)
            product = jnp.dot(centred, pmix[g], preferred_element_type=F32)
            mp[pl.ds(r, WIN), cols] = (product * pgain[:, cols]).astype(BF16)

    def pool_all(b, carry):
        pool(b)
        return carry

    def out_z(j):
        n = (z + j + R) % R
        with scope("out_z"):
            crossed(2, j)
            w = zo[n].reshape(block, zo.shape[3])
            ob[n] = lax.dot_general(ma[...], w, (((1,), (1,)), ((), ())), preferred_element_type=F32)

    def split_all():
        with scope("split_z"):
            lax.fori_loop(0, rows // 32, split_z, 0)
            tails[0].start()
            tails[1].start()

    def split_pool():
        with scope("split_y"):
            lax.fori_loop(0, rows // 32, split_y, 0)
            tails[2].start()

    def pool_now():
        with scope("tail_wait"):
            for t in tails:
                t.wait_recv()
        with scope("pool"):
            pool(0)

    def out_step(s, c):
        with scope("out_ring"):
            forward(2, s, c)
            forward(3, s, c)

    def attend_step(c, carry):
        attend_at(c + 1)
        out_step(2, c)
        return carry

    def pool_first():
        with scope("pool"):
            lax.fori_loop(1, rows // WIN, pool_all, 0)

    last_z, last_y = ready[-2:]
    before = ready[:-2] + [last_y, split_pool, pool_first, last_z, split_all]
    for c in range(NC):
        while len(before) > NC - 1 - c:
            before.pop(0)()
        out_step(1, c)
    lax.fori_loop(0, rows // WIN - 1, attend_step, 0)
    for c in range(rows // WIN - 1, NC):
        out_step(2, c)
    pool_now()
    out_step(3, 0)
    attend_at(0)
    out_step(3, 1)
    late = [lambda j=j: out_z(j) for j in order]
    for s, c in steps[2 * NC + 2 :]:
        late.pop(0)()
        out_step(s, c)
    for piece in late:
        piece()

    def exchange(n):
        return pltpu.make_async_remote_copy(
            src_ref=ob.at[n, pl.ds(theirs, own)], dst_ref=rb.at[n],
            send_sem=exs.at[0], recv_sem=exr.at[n],
            device_id={"tp": 1 - tp}, device_id_type=MESH,
        )

    def give(n, carry):
        w = yo[:, n].reshape(block, yo.shape[3])
        ob[n] += lax.dot_general(mp[...], w, (((1,), (1,)), ((), ())), preferred_element_type=F32)
        exchange(n).start()
        return carry

    with scope("out_y_wait"):
        for j in order:
            crossed(3, j)
    with scope("give"):
        lax.fori_loop(0, R, give, 0)
    with scope("keep"):
        for n in range(R):
            exchange(n).wait_recv()
            out[:, n * block : (n + 1) * block] = (ob[n, pl.ds(mine, own), :] + rb[n]).astype(BF16)

    with scope("drain"):
        tokens.wait_send()
        for t in tails:
            t.wait_send()
        for k in range(4):
            buf = streams[k][0]
            parts = (
                buf.at[pl.ds(0, R - 1), :, :, ring_cols(k)],
                buf.at[:, :, :, side_cols(k, par)],
                buf.at[0, pl.ds(0, R - 1), :, ring_cols(k)],
            )
            for i, ref in enumerate(parts):
                send(ref, sent.at[k, i], xr.at[k, 0], {"fs": (fs + 1) % nfs}).wait_send()
        ref = ob.at[:, pl.ds(theirs, own)]
        pltpu.make_async_remote_copy(
            src_ref=ref, dst_ref=rb, send_sem=exs.at[0], recv_sem=exr.at[0],
            device_id={"tp": 1 - tp}, device_id_type=MESH,
        ).wait_send()


def local(
    tokens, norm_gain, query_weight, key_matrix, value_matrix, pool_in_weight,
    head_sink_logit, pool_mix, pool_gain, attn_out_weight, pool_out_weight,
):
    R = RING
    own, width = tokens.shape[1:]
    rows = 2 * own
    block = R * SHARD
    nq = query_weight.shape[1]
    nk = key_matrix.shape[1]
    npool = pool_in_weight.shape[1]
    heads = nq // HEAD
    groups = pool_mix.shape[0]
    vmem = pl.BlockSpec(memory_space=pltpu.VMEM)
    anywhere = pl.BlockSpec(memory_space=pl.ANY)
    dma = pltpu.SemaphoreType.DMA
    result, logs = pl.pallas_call(
        kernel,
        name="mixer",
        out_shape=(
            pltpu.VMEM((own, width), BF16),
            pltpu.VMEM((heads, rows), F32),
        ),
        in_specs=[anywhere] * 11,
        out_specs=(vmem, vmem),
        scratch_shapes=[
            pltpu.VMEM((R, R, SHARD, nq + 2 * nk), BF16),
            pltpu.VMEM((R, R, SHARD, npool), BF16),
            pltpu.VMEM((R, R, SHARD, attn_out_weight.shape[0]), BF16),
            pltpu.VMEM((R, R, SHARD, pool_out_weight.shape[0]), BF16),
            pltpu.VMEM((rows, width), BF16),
            pltpu.VMEM((2, R, rows, block), BF16),
            pltpu.VMEM((rows, nq + 2 * nk), F32),
            pltpu.VMEM((rows, npool), F32),
            pltpu.VMEM((rows, nq), BF16),
            pltpu.VMEM((2, WIN + rows, nk), BF16),
            pltpu.VMEM((2, WIN + rows, nk), BF16),
            pltpu.VMEM((WIN + rows, npool), BF16),
            pltpu.VMEM((rows, nq), BF16),
            pltpu.VMEM((rows, npool), BF16),
            pltpu.VMEM((R, rows, block), F32),
            pltpu.VMEM((R, own, block), F32),
            pltpu.SMEM((2 * heads,), F32),
            pltpu.VMEM((1, width), F32),
            pltpu.VMEM((groups // 2, POOL_CH, POOL_CH), BF16),
            pltpu.VMEM((1, npool), F32),
            dma((11,)),
            dma((2,)),
            dma((4, 3)),
            dma((4, R)),
            dma((4, 2, R // 2 + 1, CHUNKS)),
            dma((4, R)),
            dma((3,)),
            dma((3,)),
            dma((1,)),
            dma((R,)),
        ],
        compiler_params=pltpu.CompilerParams(
            collective_id=0, has_side_effects=True, vmem_limit_bytes=56 * 1024 * 1024
        ),
    )(
        tokens[0],
        norm_gain[None],
        query_weight,
        key_matrix,
        value_matrix,
        pool_in_weight,
        head_sink_logit,
        pool_mix,
        pool_gain[None],
        attn_out_weight.T,
        pool_out_weight.T,
    )
    return (result[None], logs[None])


def solution(mesh):
    in_specs = (
        P("fs", ("sp", "tp"), None),
        P(),
        P("sp", "tp"),
        P("sp", "tp"),
        P("sp", "tp"),
        P("sp", "tp"),
        P(),
        P(),
        P(),
        P("tp", "sp"),
        P("tp", "sp"),
    )
    out_specs = (P("fs", ("sp", "tp"), None), P("fs", "tp", "sp"))
    return jax.shard_map(local, mesh=mesh, in_specs=in_specs, out_specs=out_specs, check_vma=False)
```

time: 92.3 us -> 81 us (0.88)
  Pallas kernels: 88.6 us -> 78.6 us
  local copies, waits for them, and re-layouts: 2.92 us -> 1.58 us
    pallas_call x1, Pallas kernels: 88.6 us -> 78.6 us  [local(): pl.pallas_call(kernel, name='mixer', out_shape=(pltpu.VMEM((own, width),...]
    unnamed x4 -> x2, local copies, waits for them, and re-layouts: 2.92 us -> 1.58 us
where the time goes in v3:
time: 81 us; the launch traced here: 80.8 us
  Pallas kernels  78.6 us (97%)
  local copies, waits for them, and re-layouts  1.58 us (2%)
    pallas_call x1, Pallas kernels, local(): pl.pallas_call(kernel, name='mixer', out_shape=(pltpu.VMEM((own, width),...  78.6 us

profile of v3, /device:TPU:1, one launch (start us, length us, event | category | flops | bytes accessed | tf_op | source)
XLA Modules:
  0.0 80.8 jit_solution(2500572332340234866)
XLA Ops:
  0.6 78.6 %mixer.1 = (bf16[256,2048]{1,0:T(8,128)(2,1)S(1)}, f32[8,512]{1,0:T(8,128)S(1)}) custom-call(bf16[256,2048]{1,0:T(8,128)(2,1)} %bitcast.9, f32[1,2048]{1,0:T(1,128)} %bitcast.12, bf16[32,512]{1,0:T(8,128)(2,1)} %wq.1, bf16[32,128]{1,0:T(8,128)(2,1)} %wk.1, bf16[32,128]{1,0:T(8,128)(2,1)} %wv.1, bf16[32,512]{1,0:T(8,128)(2,1)} %wp.1, f32[16]{0:T(128)} %sink_hbm.1, ...), custom_call_target="tpu_custom_call" | custom-call | tf_op jit(solution)/shard_map/mixer/pallas_call | solution.py:464
  79.3 1.0 %copy.15 = bf16[1,256,2048]{2,1,0:T(8,128)(2,1)} copy(bf16[1,256,2048]{2,1,0:T(8,128)(2,1)S(1)} %bitcast.7) | data formatting | bytes 2097152
  80.2 0.6 copy.16

commit v4 on v3

--- a/solution.py
+++ b/solution.py
@@ -21,7 +21,7 @@
 def kernel(
     x_hbm, gain_hbm, wq, wk, wv, wp, sink_hbm, pmix_hbm, pgain_hbm, wa, wo,
     out, lse,
-    zi, yi, zo, yo, xb, nb, accz, accy, qs, kx, vx, px, ma, mp, ob, rb, sink, gain, pmix, pgain,
+    zi, yi, zo, yo, xb, nb, accz, accy, qs, kx, vx, px, ma, mp, ob, give_b, rb, sink, gain, pmix, pgain,
     loc_sem, tok_sem, sent, p1r, bkr, xr, hls, hlr, exs, exr,
 ):
     R = RING
@@ -77,12 +77,19 @@
 
     def first(k, d):
         buf, major, minor, peer = streams[k][:4]
-        return send(buf.at[major, minor, :, ring_cols(k)], sent.at[k, 2], p1r.at[k, d], peer(d))
+        return send(buf.at[major, minor, :, ring_cols(k)], sent.at[k, 2], p1r.at[k, kind(k, d)], peer(d))
+
+    def kind(k, d):
+        return int(k > 1 and d % R in (2, R - 2))
+
+    def arrived(k, which, n):
+        ref = streams[k][0].at[0, pl.ds(0, n), :, ring_cols(k)]
+        send(ref, sent.at[k, 2], p1r.at[k, which], {"fs": (fs + 1) % nfs}).wait_recv()
 
     def second(k, d, hop):
         buf, major, minor, peer = streams[k][:4]
         ref = buf.at[major, (minor - d + R) % R, :, ring_cols(k)]
-        return send(ref, sent.at[k, 2], p1r.at[k, (d + hop) % R], peer(hop))
+        return send(ref, sent.at[k, 2], p1r.at[k, kind(k, d + hop)], peer(hop))
 
     FURTHER = ((2, 1), (R - 2, -1), (2, 2))
 
@@ -94,7 +101,7 @@
         buf, major, _, _, peer = streams[k][:5]
         sign = SIGN[way]
         ref = buf.at[(major - sign * (s - 1) + R) % R, piece_of(k, c), :, ring_cols(k)]
-        return send(ref, sent.at[k, 0], bkr.at[k, way, s, c], peer(sign))
+        return send(ref, sent.at[k, 0], bkr.at[k, s - 1, c], peer(sign))
 
     def is_sent(way, s, c):
         return s < half or (s == half and (c < NC // 2) == (way == 0))
@@ -107,24 +114,28 @@
         buf, major = streams[k][:2]
         ref = buf.at[(major + j + R) % R, piece_of(k, c), :, side_cols(k, par)]
         step = 1 + (nfs - 2) * (c // (NC // 2))
-        return send(ref, sent.at[k, 1], xr.at[k, j % R], {"fs": (fs + step) % nfs})
+        return send(ref, sent.at[k, 1], xr.at[k, j_abs(j)], {"fs": (fs + step) % nfs})
+
+    def j_abs(j):
+        return max(j, -j)
 
     def crossed(k, j):
-        buf, major = streams[k][:2]
-        ref = buf.at[(major + j + R) % R, :, :, side_cols(k, 1 - par)]
-        send(ref, sent.at[k, 1], xr.at[k, j % R], {"fs": (fs + 1) % nfs}).wait_recv()
+        if j >= 0:
+            ref = streams[k][0].at[pl.ds(0, 2 if 0 < j < half else 1), :, :, side_cols(k, 1 - par)]
+            send(ref, sent.at[k, 1], xr.at[k, j], {"fs": (fs + 1) % nfs}).wait_recv()
 
     def own_piece(k, c):
         for way in (0, 1):
             bulk(k, way, 1, c).start()
 
     def forward(k, s, c):
-        for way in (0, 1):
-            if is_sent(way, s, c):
-                bulk(k, way, s, c).wait_recv()
-                if is_sent(way, s + 1, c):
-                    bulk(k, way, s + 1, c).start()
-                cross(k, -SIGN[way] * s, c).start()
+        ways = [way for way in (0, 1) if is_sent(way, s, c)]
+        ref = streams[k][0].at[0, pl.ds(0, len(ways) * chunk), :, ring_cols(k)]
+        send(ref, sent.at[k, 0], bkr.at[k, s - 1, c], {"fs": (fs + 1) % nfs}).wait_recv()
+        for way in ways:
+            if is_sent(way, s + 1, c):
+                bulk(k, way, s + 1, c).start()
+            cross(k, -SIGN[way] * s, c).start()
 
     barrier = pltpu.get_barrier_semaphore()
     peers = [{"tp": 1 - tp}]
@@ -147,17 +158,17 @@
     place(wk, zi.at[a, b, :, pl.ds(nq // 2, nk)])
     place(wv, zi.at[a, b, :, pl.ds(nq // 2 + nk, nk)])
     place(wp.at[:, ring_cols(1)], yi.at[b, a, :, ring_cols(1)])
+    place(x_hbm, xb.at[pl.ds(mine, own)])
+    place(gain_hbm, gain)
     place(wa.at[:, ring_cols(2)], zo.at[z, y, :, ring_cols(2)])
     place(wo.at[:, ring_cols(3)], yo.at[y, z, :, ring_cols(3)])
-    place(x_hbm, xb.at[pl.ds(mine, own)])
-    place(gain_hbm, gain)
     place(sink_hbm, sink)
     place(pmix_hbm.at[pl.ds(tp * pmix.shape[0], pmix.shape[0])], pmix)
     place(pgain_hbm.at[:, pl.ds(pl.multiple_of(tp * npool, 128), npool)], pgain)
 
     with scope("barrier"):
         pl.semaphore_wait(barrier, len(peers))
-        for copy in local:
+        for copy in local[:4]:
             copy.wait()
 
     tokens = send(xb.at[pl.ds(mine, own)], tok_sem.at[0], tok_sem.at[1], {"tp": 1 - tp})
@@ -205,6 +216,8 @@
     for d in (half, 3, R - 3, 2, R - 2, 1, R - 1):
         first(0, d).start()
         first(1, d).start()
+    for copy in local[4:]:
+        copy.wait()
     tokens.start()
     with scope("norm"):
         lax.fori_loop(0, rows // 32, zero, 0)
@@ -218,8 +231,7 @@
         norm(theirs)
     with scope("first"):
         for k in (0, 1):
-            for d in range(1, R):
-                first(k, d).wait_recv()
+            arrived(k, 0, R - 1)
         for c in range(NC):
             for k in (0, 1):
                 own_piece(k, c)
@@ -236,35 +248,32 @@
         if i == 1:
             with scope("second"):
                 for k in (2, 3):
-                    first(k, 2).wait_recv()
-                    first(k, R - 2).wait_recv()
+                    arrived(k, 1, 2)
                     for d, hop in FURTHER:
                         second(k, d, hop).start()
         if i == 3 * NC - 1:
             with scope("own_out"):
                 for k in (2, 3):
-                    for d in range(1, R):
-                        if d not in (2, R - 2):
-                            first(k, d).wait_recv()
+                    arrived(k, 0, R - 3)
                     for n in range(NC):
                         own_piece(k, n)
-        if i in (2, 3) or i > NC:
+        for _ in range(4 if i == 3 * NC - 1 else i in (4, 5, 7, 8, 9, 10)):
             ready.pop(0)()
     for k in (2, 3):
         for c in range(NC):
             cross(k, 0, c).start()
 
     def split_z(i, carry):
-        r = pl.multiple_of(i * 32, 32)
-        e = pl.multiple_of(WIN + i * 32, 32)
+        r = pl.multiple_of(i * 128, 128)
+        e = pl.multiple_of(WIN + i * 128, 128)
         for p in range(heads // 2):
             at = p * 128 if p < heads // 4 else p * 128 + 2 * nk
-            q = accz[pl.ds(r, 32), at : at + 128] * (HEAD ** (-0.5))
-            qs[pl.ds(r, 32), p * 128 : (p + 1) * 128] = q.astype(BF16)
+            q = accz[pl.ds(r, 128), at : at + 128] * (HEAD ** (-0.5))
+            qs[pl.ds(r, 128), p * 128 : (p + 1) * 128] = q.astype(BF16)
         for ref, at in ((kx, nq // 2), (vx, nq // 2 + nk)):
-            t = accz[pl.ds(r, 32), at : at + nk]
-            ref[0, pl.ds(e, 32), :] = t.astype(BF16)
-            ref[1, pl.ds(e, 32), :] = pltpu.roll(t, HEAD, 1).astype(BF16)
+            t = accz[pl.ds(r, 128), at : at + nk]
+            ref[0, pl.ds(e, 128), :] = t.astype(BF16)
+            ref[1, pl.ds(e, 128), :] = pltpu.roll(t, HEAD, 1).astype(BF16)
         return carry
 
     def split_y(i, carry):
@@ -276,8 +285,8 @@
     def tail(i, ref, n):
         src, dst = pl.ds(WIN + rows - n, n), pl.ds(WIN - n, n)
         return pltpu.make_async_remote_copy(
-            src_ref=ref.at[src] if i == 2 else ref.at[:, src],
-            dst_ref=ref.at[dst] if i == 2 else ref.at[:, dst],
+            src_ref=ref.at[src] if i == 2 else ref.at[0, src],
+            dst_ref=ref.at[dst] if i == 2 else ref.at[0, dst],
             send_sem=hls.at[i], recv_sem=hlr.at[i],
             device_id={"sp": (sp + 1) % (R * R)}, device_id_type=MESH,
         )
@@ -293,28 +302,32 @@
         left = j < HEAD
         halves = (jnp.where(left, 1.0, 0.0).astype(BF16), jnp.where(left, 0.0, 1.0).astype(BF16))
         logs = jnp.zeros((WIN, 128), F32)
-        for p in range(heads // 2):
-            pair = qs[pl.ds(r, WIN), p * 128 : (p + 1) * 128]
-            outs = []
-            for odd in (0, 1):
-                h = 2 * p + odd
-                turned = odd ^ (h // (heads // 2))
+        width = heads // 2
+        for g in (0, 1):
+            scores = []
+            for h in range(g * width, (g + 1) * width):
+                pair = qs[pl.ds(r, WIN), h // 2 * 128 : h // 2 * 128 + 128]
                 score = lax.dot_general(
-                    pair * halves[odd], kx[turned, pl.ds(r, 2 * WIN), :], (((1,), (1,)), ((), ())),
+                    pair * halves[h % 2], kx[h % 2 ^ g, pl.ds(r, 2 * WIN), :], (((1,), (1,)), ((), ())),
                     preferred_element_type=F32,
                 )
-                score = jnp.where(older, score[:, :WIN] + missing, score[:, WIN:])
-                s = sink[tp * heads + h]
-                top = jnp.maximum(jnp.max(score, axis=1, keepdims=True), s)
-                weight = jnp.exp(score - top)
-                total = jnp.sum(weight, axis=1, keepdims=True) + jnp.exp(s - top)
-                probs = weight * (1.0 / total)
+                scores.append(jnp.where(older, score[:, :WIN] + missing, score[:, WIN:]))
+            sinks = [sink[tp * heads + g * width + n] for n in range(width)]
+            tops = [jnp.maximum(jnp.max(v, axis=1, keepdims=True), s) for v, s in zip(scores, sinks)]
+            weights = [jnp.exp(v - t) for v, t in zip(scores, tops)]
+            totals = [jnp.sum(v, axis=1, keepdims=True) + jnp.exp(s - t) for v, s, t in zip(weights, sinks, tops)]
+            outs = []
+            for n in range(width):
+                probs = weights[n] * (1.0 / totals[n])
                 band = jnp.concatenate(
                     [jnp.where(older, probs, 0.0).astype(BF16), jnp.where(older, 0.0, probs).astype(BF16)], axis=1
                 )
-                outs.append(jnp.dot(band, vx[turned, pl.ds(r, 2 * WIN), :], preferred_element_type=F32))
-                logs = jnp.where(j == h, top + jnp.log(total), logs)
-            ma[pl.ds(r, WIN), p * 128 : (p + 1) * 128] = jnp.where(left, outs[0], outs[1]).astype(BF16)
+                outs.append(jnp.dot(band, vx[n % 2 ^ g, pl.ds(r, 2 * WIN), :], preferred_element_type=F32))
+            for n in range(width):
+                logs = jnp.where(j == g * width + n, tops[n] + jnp.log(totals[n]), logs)
+            for n in range(0, width, 2):
+                at = (g * width + n) // 2 * 128
+                ma[pl.ds(r, WIN), at : at + 128] = jnp.where(left, outs[n], outs[n + 1]).astype(BF16)
         lse[:, pl.ds(r, WIN)] = jnp.transpose(logs)[:heads, :]
 
     def attend_at(b):
@@ -343,16 +356,23 @@
         pool(b)
         return carry
 
-    def out_z(j):
-        n = (z + j + R) % R
-        with scope("out_z"):
-            crossed(2, j)
+    def out_z(t, carry):
+        for n in range(R // 2):
+            @pl.when(t == n)
+            def _():
+                for step in steps[2 * NC + 2 + max(n, 2 * n - 2) :][: 1 if n < 2 else 2]:
+                    out_step(*step)
+                crossed(2, n + 1)
+
+        for i in (2 * t, 2 * t + 1):
+            n = (z + (i + 1) // 2 * (2 * (i % 2) - 1) + R) % R
             w = zo[n].reshape(block, zo.shape[3])
             ob[n] = lax.dot_general(ma[...], w, (((1,), (1,)), ((), ())), preferred_element_type=F32)
+        return carry
 
     def split_all():
         with scope("split_z"):
-            lax.fori_loop(0, rows // 32, split_z, 0)
+            lax.fori_loop(0, rows // 128, split_z, 0)
             tails[0].start()
             tails[1].start()
 
@@ -365,6 +385,8 @@
         with scope("tail_wait"):
             for t in tails:
                 t.wait_recv()
+            for ref in (kx, vx):
+                ref[1, 0:WIN, :] = pltpu.roll(ref[0, 0:WIN, :].astype(F32), HEAD, 1).astype(BF16)
         with scope("pool"):
             pool(0)
 
@@ -375,7 +397,11 @@
 
     def attend_step(c, carry):
         attend_at(c + 1)
-        out_step(2, c)
+        for n, step in enumerate(((2, 2), (2, 3), (3, 0))):
+            @pl.when(c == n)
+            def _():
+                out_step(*step)
+
         return carry
 
     def pool_first():
@@ -383,47 +409,52 @@
             lax.fori_loop(1, rows // WIN, pool_all, 0)
 
     last_z, last_y = ready[-2:]
-    before = ready[:-2] + [last_y, split_pool, pool_first, last_z, split_all]
-    for c in range(NC):
-        while len(before) > NC - 1 - c:
-            before.pop(0)()
-        out_step(1, c)
+    out_step(1, 0)
+    for n, piece in enumerate(ready[:-2]):
+        piece()
+        if n % 2:
+            out_step(1, 1 + n // 2)
+    last_y()
+    split_pool()
+    out_step(1, 3)
+    pool_first()
+    out_step(2, 0)
+    last_z()
+    split_all()
+    out_step(2, 1)
     lax.fori_loop(0, rows // WIN - 1, attend_step, 0)
-    for c in range(rows // WIN - 1, NC):
-        out_step(2, c)
     pool_now()
-    out_step(3, 0)
+    out_step(3, 1)
     attend_at(0)
-    out_step(3, 1)
-    late = [lambda j=j: out_z(j) for j in order]
-    for s, c in steps[2 * NC + 2 :]:
-        late.pop(0)()
-        out_step(s, c)
-    for piece in late:
-        piece()
+    with scope("out_z"):
+        crossed(2, 0)
+        lax.fori_loop(0, R // 2, out_z, 0)
 
     def exchange(n):
         return pltpu.make_async_remote_copy(
-            src_ref=ob.at[n, pl.ds(theirs, own)], dst_ref=rb.at[n],
+            src_ref=give_b.at[pl.ds(2 * n, 2)], dst_ref=rb.at[pl.ds(2 * n, 2)],
             send_sem=exs.at[0], recv_sem=exr.at[n],
             device_id={"tp": 1 - tp}, device_id_type=MESH,
         )
 
-    def give(n, carry):
-        w = yo[:, n].reshape(block, yo.shape[3])
-        ob[n] += lax.dot_general(mp[...], w, (((1,), (1,)), ((), ())), preferred_element_type=F32)
-        exchange(n).start()
+    def give(m, carry):
+        for n in (2 * m, 2 * m + 1):
+            w = yo[:, n].reshape(block, yo.shape[3])
+            ob[n] += lax.dot_general(mp[...], w, (((1,), (1,)), ((), ())), preferred_element_type=F32)
+            give_b[n] = ob[n, pl.ds(theirs, own), :].astype(BF16)
+        exchange(m).start()
         return carry
 
     with scope("out_y_wait"):
         for j in order:
             crossed(3, j)
     with scope("give"):
-        lax.fori_loop(0, R, give, 0)
+        lax.fori_loop(0, R // 2, give, 0)
     with scope("keep"):
         for n in range(R):
-            exchange(n).wait_recv()
-            out[:, n * block : (n + 1) * block] = (ob[n, pl.ds(mine, own), :] + rb[n]).astype(BF16)
+            if n % 2 == 0:
+                exchange(n // 2).wait_recv()
+            out[:, n * block : (n + 1) * block] = (ob[n, pl.ds(mine, own), :] + rb[n].astype(F32)).astype(BF16)
 
     with scope("drain"):
         tokens.wait_send()
@@ -438,9 +469,8 @@
             )
             for i, ref in enumerate(parts):
                 send(ref, sent.at[k, i], xr.at[k, 0], {"fs": (fs + 1) % nfs}).wait_send()
-        ref = ob.at[:, pl.ds(theirs, own)]
         pltpu.make_async_remote_copy(
-            src_ref=ref, dst_ref=rb, send_sem=exs.at[0], recv_sem=exr.at[0],
+            src_ref=give_b, dst_ref=rb, send_sem=exs.at[0], recv_sem=exr.at[0],
             device_id={"tp": 1 - tp}, device_id_type=MESH,
         ).wait_send()
 
@@ -486,7 +516,8 @@
             pltpu.VMEM((rows, nq), BF16),
             pltpu.VMEM((rows, npool), BF16),
             pltpu.VMEM((R, rows, block), F32),
-            pltpu.VMEM((R, own, block), F32),
+            pltpu.VMEM((R, own, block), BF16),
+            pltpu.VMEM((R, own, block), BF16),
             pltpu.SMEM((2 * heads,), F32),
             pltpu.VMEM((1, width), F32),
             pltpu.VMEM((groups // 2, POOL_CH, POOL_CH), BF16),
@@ -494,13 +525,13 @@
             dma((11,)),
             dma((2,)),
             dma((4, 3)),
-            dma((4, R)),
-            dma((4, 2, R // 2 + 1, CHUNKS)),
-            dma((4, R)),
+            dma((4, 2)),
+            dma((4, R // 2, CHUNKS)),
+            dma((4, R // 2 + 1)),
             dma((3,)),
             dma((3,)),
             dma((1,)),
-            dma((R,)),
+            dma((R // 2,)),
         ],
         compiler_params=pltpu.CompilerParams(
             collective_id=0, has_side_effects=True, vmem_limit_bytes=56 * 1024 * 1024

time: 81 us -> 76 us (0.938)
  Pallas kernels: 78.6 us -> 73.7 us
    pallas_call x1, Pallas kernels: 78.6 us -> 73.7 us  [local(): pl.pallas_call(kernel, name='mixer', out_shape=(pltpu.VMEM((own, width),...]
where the time goes in v4:
time: 76 us; the launch traced here: 75.9 us
  Pallas kernels  73.7 us (97%)
  local copies, waits for them, and re-layouts  1.58 us (2%)
    pallas_call x1, Pallas kernels, local(): pl.pallas_call(kernel, name='mixer', out_shape=(pltpu.VMEM((own, width),...  73.7 us
    unnamed x2, local copies, waits for them, and re-layouts  1.58 us

profile of v4, /device:TPU:1, one launch (start us, length us, event | category | flops | bytes accessed | tf_op | source)
XLA Modules:
  0.0 75.9 jit_solution(15733854828928347301)
XLA Ops:
  0.6 73.7 %mixer.1 = (bf16[256,2048]{1,0:T(8,128)(2,1)S(1)}, f32[8,512]{1,0:T(8,128)S(1)}) custom-call(bf16[256,2048]{1,0:T(8,128)(2,1)} %bitcast.9, f32[1,2048]{1,0:T(1,128)} %bitcast.12, bf16[32,512]{1,0:T(8,128)(2,1)} %wq.1, bf16[32,128]{1,0:T(8,128)(2,1)} %wk.1, bf16[32,128]{1,0:T(8,128)(2,1)} %wv.1, bf16[32,512]{1,0:T(8,128)(2,1)} %wp.1, f32[16]{0:T(128)} %sink_hbm.1, ...), custom_call_target="tpu_custom_call" | custom-call | tf_op jit(solution)/shard_map/mixer/pallas_call | solution.py:494
  74.3 1.0 %copy.15 = bf16[1,256,2048]{2,1,0:T(8,128)(2,1)} copy(bf16[1,256,2048]{2,1,0:T(8,128)(2,1)S(1)} %bitcast.7) | data formatting | bytes 2097152
  75.3 0.6 copy.16

commit v5 on v4

--- a/solution.py
+++ b/solution.py
@@ -16,6 +16,7 @@
 BF16 = jnp.bfloat16
 MESH = pl.DeviceIdType.MESH
 SIGN = (1, -1)
+INWARD = (3, 1, 2, 0)
 
 
 def kernel(
@@ -77,19 +78,19 @@
 
     def first(k, d):
         buf, major, minor, peer = streams[k][:4]
-        return send(buf.at[major, minor, :, ring_cols(k)], sent.at[k, 2], p1r.at[k, kind(k, d)], peer(d))
+        return send(buf.at[major, minor, :, ring_cols(k)], sent.at[k, 2], p1r.at[kind(k, d)], peer(d))
 
     def kind(k, d):
-        return int(k > 1 and d % R in (2, R - 2))
+        return 2 * R + 2 * (k - 2) + int(d % R in (2, R - 2)) if k > 1 else k * R + d
 
     def arrived(k, which, n):
         ref = streams[k][0].at[0, pl.ds(0, n), :, ring_cols(k)]
-        send(ref, sent.at[k, 2], p1r.at[k, which], {"fs": (fs + 1) % nfs}).wait_recv()
+        send(ref, sent.at[k, 2], p1r.at[2 * R + 2 * (k - 2) + which], {"fs": (fs + 1) % nfs}).wait_recv()
 
     def second(k, d, hop):
         buf, major, minor, peer = streams[k][:4]
         ref = buf.at[major, (minor - d + R) % R, :, ring_cols(k)]
-        return send(ref, sent.at[k, 2], p1r.at[k, kind(k, d + hop)], peer(hop))
+        return send(ref, sent.at[k, 2], p1r.at[kind(k, d + hop)], peer(hop))
 
     FURTHER = ((2, 1), (R - 2, -1), (2, 2))
 
@@ -135,7 +136,17 @@
         for way in ways:
             if is_sent(way, s + 1, c):
                 bulk(k, way, s + 1, c).start()
-            cross(k, -SIGN[way] * s, c).start()
+            if k < 2 or s < half:
+                cross(k, -SIGN[way] * s, c).start()
+
+    def late(k):
+        buf, major, _, _, peer = streams[k][:5]
+        for way in (0, 1):
+            sign = SIGN[way]
+            for c in range(NC):
+                if is_sent(way, half, c):
+                    ref = buf.at[(major - sign * (half - 1) + R) % R, piece_of(k, c), :, side_cols(k, 1 - par)]
+                    send(ref, sent.at[k, 1], xr.at[k, half], peer(sign)).start()
 
     barrier = pltpu.get_barrier_semaphore()
     peers = [{"tp": 1 - tp}]
@@ -230,10 +241,15 @@
         tokens.wait_recv()
         norm(theirs)
     with scope("first"):
-        for k in (0, 1):
-            arrived(k, 0, R - 1)
-        for c in range(NC):
+        for c in INWARD:
             for k in (0, 1):
+                minor = streams[k][2]
+                start = (minor // chunk + c + (c // 2) * (5 - 2 * c)) % NC * chunk
+                if c == 0:
+                    first(k, (2 * (minor % 2) + R - 1) % R).wait_recv()
+                else:
+                    first(k, (minor - start + R) % R).wait_recv()
+                    first(k, (minor - start - 1 + R) % R).wait_recv()
                 own_piece(k, c)
                 cross(k, 0, c).start()
 
@@ -241,16 +257,16 @@
     ready = [lambda j=j, f=f: f(j) for j in order for f in (in_z, in_y)]
     steps = [(s, c) for s in range(1, half) for c in range(NC)]
     steps += [(half, c) for c in (0, 2, 1, 3)]
-    for i, (s, c) in enumerate(steps):
+    in_steps = [(s, c) for s in range(1, half + 1) for c in INWARD]
+    with scope("second"):
+        for k in (2, 3):
+            arrived(k, 1, 2)
+            for d, hop in FURTHER:
+                second(k, d, hop).start()
+    for i, (s, c) in enumerate(in_steps):
         with scope("in_ring"):
             forward(0, s, c)
             forward(1, s, c)
-        if i == 1:
-            with scope("second"):
-                for k in (2, 3):
-                    arrived(k, 1, 2)
-                    for d, hop in FURTHER:
-                        second(k, d, hop).start()
         if i == 3 * NC - 1:
             with scope("own_out"):
                 for k in (2, 3):
@@ -360,9 +376,14 @@
         for n in range(R // 2):
             @pl.when(t == n)
             def _():
+                if n == 2:
+                    for k in (2, 3):
+                        crossed(k, half - 1)
+                        late(k)
                 for step in steps[2 * NC + 2 + max(n, 2 * n - 2) :][: 1 if n < 2 else 2]:
                     out_step(*step)
-                crossed(2, n + 1)
+                if n != 2:
+                    crossed(2, n + 1)
 
         for i in (2 * t, 2 * t + 1):
             n = (z + (i + 1) // 2 * (2 * (i % 2) - 1) + R) % R
@@ -446,7 +467,7 @@
         return carry
 
     with scope("out_y_wait"):
-        for j in order:
+        for j in (0, 1, 2, half):
             crossed(3, j)
     with scope("give"):
         lax.fori_loop(0, R // 2, give, 0)
@@ -473,6 +494,19 @@
             src_ref=give_b, dst_ref=rb, send_sem=exs.at[0], recv_sem=exr.at[0],
             device_id={"tp": 1 - tp}, device_id_type=MESH,
         ).wait_send()
+
+
+def leave(result, logs, result_hbm, logs_hbm, sem):
+    copies = []
+    rows = result.shape[0] // 4
+    for n in range(4):
+        part = pl.ds(n * rows, rows)
+        copies.append(pltpu.make_async_copy(result.at[part], result_hbm.at[part], sem.at[n]))
+    copies.append(pltpu.make_async_copy(logs, logs_hbm, sem.at[4]))
+    for copy in copies:
+        copy.start()
+    for copy in copies:
+        copy.wait()
 
 
 def local(
@@ -525,7 +559,7 @@
             dma((11,)),
             dma((2,)),
             dma((4, 3)),
-            dma((4, 2)),
+            dma((2 * R + 4,)),
             dma((4, R // 2, CHUNKS)),
             dma((4, R // 2 + 1)),
             dma((3,)),
@@ -549,6 +583,18 @@
         attn_out_weight.T,
         pool_out_weight.T,
     )
+    result, logs = pl.pallas_call(
+        leave,
+        name="leave",
+        out_shape=(
+            jax.ShapeDtypeStruct((own, width), BF16),
+            jax.ShapeDtypeStruct((heads, rows), F32),
+        ),
+        in_specs=[vmem, vmem],
+        out_specs=(anywhere, anywhere),
+        scratch_shapes=[dma((5,))],
+        compiler_params=pltpu.CompilerParams(vmem_limit_bytes=4 * 1024 * 1024),
+    )(result, logs)
     return (result[None], logs[None])
 
 

time: 76 us -> 72.8 us (0.958)
  Pallas kernels: 73.7 us -> 72 us
  local copies, waits for them, and re-layouts: 1.58 us -> 0 us
    pallas_call x1, Pallas kernels: 73.7 us -> 71 us  [local(): pl.pallas_call(kernel, name='mixer', out_shape=(pltpu.VMEM((own, width),...]
    unnamed x2 -> x0, local copies, waits for them, and re-layouts: 1.58 us -> none
    pallas_call x0 -> x1, Pallas kernels: none -> 1.01 us  [local(): pl.pallas_call(leave, name='leave', out_shape=(jax.ShapeDtypeStruct((own,...]
where the time goes in v5:
time: 72.8 us; the launch traced here: 72.7 us
  Pallas kernels  72 us (99%)
    pallas_call x1, Pallas kernels, local(): pl.pallas_call(kernel, name='mixer', out_shape=(pltpu.VMEM((own, width),...  71 us

profile of v5, /device:TPU:1, one launch (start us, length us, event | category | flops | bytes accessed | tf_op | source)
XLA Modules:
  0.0 72.7 jit_solution(13115392227057349217)
XLA Ops:
  0.6 71.0 %mixer.1 = (bf16[256,2048]{1,0:T(8,128)(2,1)S(1)}, f32[8,512]{1,0:T(8,128)S(1)}) custom-call(bf16[256,2048]{1,0:T(8,128)(2,1)} %bitcast.7, f32[1,2048]{1,0:T(1,128)} %bitcast.10, bf16[32,512]{1,0:T(8,128)(2,1)} %wq.1, bf16[32,128]{1,0:T(8,128)(2,1)} %wk.1, bf16[32,128]{1,0:T(8,128)(2,1)} %wv.1, bf16[32,512]{1,0:T(8,128)(2,1)} %wp.1, f32[16]{0:T(128)} %sink_hbm.1, ...), custom_call_target="tpu_custom_call" | custom-call | tf_op jit(solution)/shard_map/mixer/pallas_call | solution.py:528
  71.7 1.0 %leave.1 = (bf16[256,2048]{1,0:T(8,128)(2,1)}, f32[8,512]{1,0:T(8,128)}) custom-call(bf16[256,2048]{1,0:T(8,128)(2,1)S(1)} %get-tuple-element.6.result, f32[8,512]{1,0:T(8,128)S(1)} %get-tuple-element.7.logs), custom_call_target="tpu_custom_call" | custom-call | tf_op jit(solution)/shard_map/leave/pallas_call | solution.py:586

commit v6 on v5

--- a/solution.py
+++ b/solution.py
@@ -16,6 +16,7 @@
 BF16 = jnp.bfloat16
 MESH = pl.DeviceIdType.MESH
 SIGN = (1, -1)
+WIDE = (3, 0)
 INWARD = (3, 1, 2, 0)
 
 
@@ -101,28 +102,36 @@
     def bulk(k, way, s, c):
         buf, major, _, _, peer = streams[k][:5]
         sign = SIGN[way]
-        ref = buf.at[(major - sign * (s - 1) + R) % R, piece_of(k, c), :, ring_cols(k)]
+        ref = buf.at[(major - sign * (s - 1) + R) % R, piece_of(k, c), :, across_cols(k, c, par, False)]
         return send(ref, sent.at[k, 0], bkr.at[k, s - 1, c], peer(sign))
 
     def is_sent(way, s, c):
         return s < half or (s == half and (c < NC // 2) == (way == 0))
 
+    def across_cols(k, c, p, own_side, mine=False):
+        side, middle = streams[k][5:]
+        more = side if k == 1 and c in WIDE and not mine else 0
+        width = side + more if own_side else side + middle - more
+        return pl.ds(pl.multiple_of(p * (2 * side + middle - width), 128), width)
+
     def side_cols(k, p):
-        side, middle = streams[k][5:]
-        return pl.ds(pl.multiple_of(p * (side + middle), 128), side)
+        return across_cols(k, NC, p, True)
 
     def cross(k, j, c):
         buf, major = streams[k][:2]
-        ref = buf.at[(major + j + R) % R, piece_of(k, c), :, side_cols(k, par)]
+        ref = buf.at[(major + j + R) % R, piece_of(k, c), :, across_cols(k, c, par, True, j == 0)]
         step = 1 + (nfs - 2) * (c // (NC // 2))
-        return send(ref, sent.at[k, 1], xr.at[k, j_abs(j)], {"fs": (fs + step) % nfs})
+        return send(ref, sent.at[k, 3 if k == 1 and j == 0 else 1], xr.at[k, j_abs(j)], {"fs": (fs + step) % nfs})
 
     def j_abs(j):
         return max(j, -j)
 
     def crossed(k, j):
         if j >= 0:
-            ref = streams[k][0].at[pl.ds(0, 2 if 0 < j < half else 1), :, :, side_cols(k, 1 - par)]
+            blocks = 2 if 0 < j < half else 1
+            ref = streams[k][0].at[pl.ds(0, blocks), :, :, side_cols(k, 1 - par)]
+            if k == 1 and j > 0:
+                ref = streams[k][0].at[0, pl.ds(0, 3 * blocks)]
             send(ref, sent.at[k, 1], xr.at[k, j], {"fs": (fs + 1) % nfs}).wait_recv()
 
     def own_piece(k, c):
@@ -131,7 +140,7 @@
 
     def forward(k, s, c):
         ways = [way for way in (0, 1) if is_sent(way, s, c)]
-        ref = streams[k][0].at[0, pl.ds(0, len(ways) * chunk), :, ring_cols(k)]
+        ref = streams[k][0].at[0, pl.ds(0, len(ways) * chunk), :, across_cols(k, c, par, False)]
         send(ref, sent.at[k, 0], bkr.at[k, s - 1, c], {"fs": (fs + 1) % nfs}).wait_recv()
         for way in ways:
             if is_sent(way, s + 1, c):
@@ -488,6 +497,13 @@
                 buf.at[:, :, :, side_cols(k, par)],
                 buf.at[0, pl.ds(0, R - 1), :, ring_cols(k)],
             )
+            if k == 1:
+                parts = (
+                    buf.at[pl.ds(0, 5), pl.ds(0, R - 1)],
+                    buf.at[pl.ds(0, 3), pl.ds(0, R - 1)],
+                    parts[2],
+                    buf.at[0, :, :, side_cols(k, par)],
+                )
             for i, ref in enumerate(parts):
                 send(ref, sent.at[k, i], xr.at[k, 0], {"fs": (fs + 1) % nfs}).wait_send()
         pltpu.make_async_remote_copy(
@@ -558,7 +574,7 @@
             pltpu.VMEM((1, npool), F32),
             dma((11,)),
             dma((2,)),
-            dma((4, 3)),
+            dma((4, 4)),
             dma((2 * R + 4,)),
             dma((4, R // 2, CHUNKS)),
             dma((4, R // 2 + 1)),

time: 72.8 us -> 71.9 us (0.988)
  Pallas kernels: 72 us -> 71.2 us
    pallas_call x1, Pallas kernels: 71 us -> 70.2 us  [local(): pl.pallas_call(kernel, name='mixer', out_shape=(pltpu.VMEM((own, width),...]
where the time goes in v6:
time: 71.9 us; the launch traced here: 71.8 us
  Pallas kernels  71.2 us (99%)
    pallas_call x1, Pallas kernels, local(): pl.pallas_call(kernel, name='mixer', out_shape=(pltpu.VMEM((own, width),...  70.2 us

profile of v6, /device:TPU:1, one launch (start us, length us, event | category | flops | bytes accessed | tf_op | source)
XLA Modules:
  0.0 71.8 jit_solution(1299140679941017021)
XLA Ops:
  0.6 70.2 %mixer.1 = (bf16[256,2048]{1,0:T(8,128)(2,1)S(1)}, f32[8,512]{1,0:T(8,128)S(1)}) custom-call(bf16[256,2048]{1,0:T(8,128)(2,1)} %bitcast.7, f32[1,2048]{1,0:T(1,128)} %bitcast.10, bf16[32,512]{1,0:T(8,128)(2,1)} %wq.1, bf16[32,128]{1,0:T(8,128)(2,1)} %wk.1, bf16[32,128]{1,0:T(8,128)(2,1)} %wv.1, bf16[32,512]{1,0:T(8,128)(2,1)} %wp.1, f32[16]{0:T(128)} %sink_hbm.1, ...), custom_call_target="tpu_custom_call" | custom-call | tf_op jit(solution)/shard_map/mixer/pallas_call | solution.py:544
  70.8 1.0 %leave.1 = (bf16[256,2048]{1,0:T(8,128)(2,1)}, f32[8,512]{1,0:T(8,128)}) custom-call(bf16[256,2048]{1,0:T(8,128)(2,1)S(1)} %get-tuple-element.6.result, f32[8,512]{1,0:T(8,128)S(1)} %get-tuple-element.7.logs), custom_call_target="tpu_custom_call" | custom-call | tf_op jit(solution)/shard_map/leave/pallas_call | solution.py:602

commit v7 on v6

--- a/solution.py
+++ b/solution.py
@@ -103,7 +103,7 @@
         buf, major, _, _, peer = streams[k][:5]
         sign = SIGN[way]
         ref = buf.at[(major - sign * (s - 1) + R) % R, piece_of(k, c), :, across_cols(k, c, par, False)]
-        return send(ref, sent.at[k, 0], bkr.at[k, s - 1, c], peer(sign))
+        return send(ref, sent.at[k, 0], bkr.at[min(k, 2), s - 1, c], peer(sign))
 
     def is_sent(way, s, c):
         return s < half or (s == half and (c < NC // 2) == (way == 0))
@@ -140,8 +140,10 @@
 
     def forward(k, s, c):
         ways = [way for way in (0, 1) if is_sent(way, s, c)]
-        ref = streams[k][0].at[0, pl.ds(0, len(ways) * chunk), :, across_cols(k, c, par, False)]
-        send(ref, sent.at[k, 0], bkr.at[k, s - 1, c], {"fs": (fs + 1) % nfs}).wait_recv()
+        if k < 3:
+            streams_waited = 1 if k < 2 else 2
+            ref = streams[k][0].at[0, pl.ds(0, streams_waited * len(ways) * chunk), :, across_cols(k, c, par, False)]
+            send(ref, sent.at[k, 0], bkr.at[k, s - 1, c], {"fs": (fs + 1) % nfs}).wait_recv()
         for way in ways:
             if is_sent(way, s + 1, c):
                 bulk(k, way, s + 1, c).start()
@@ -576,7 +578,7 @@
             dma((2,)),
             dma((4, 4)),
             dma((2 * R + 4,)),
-            dma((4, R // 2, CHUNKS)),
+            dma((3, R // 2, CHUNKS)),
             dma((4, R // 2 + 1)),
             dma((3,)),
             dma((3,)),

time: 71.9 us -> 72.6 us (level)
  no operation moved by 1% of the time
where the time goes in v7:
time: 72.6 us; the launch traced here: 72.5 us
  Pallas kernels  71.8 us (99%)
    pallas_call x1, Pallas kernels, local(): pl.pallas_call(kernel, name='mixer', out_shape=(pltpu.VMEM((own, width),...  70.8 us

profile of v7, /device:TPU:1, one launch (start us, length us, event | category | flops | bytes accessed | tf_op | source)
XLA Modules:
  0.0 72.5 jit_solution(6875201530338390040)
XLA Ops:
  0.6 70.8 %mixer.1 = (bf16[256,2048]{1,0:T(8,128)(2,1)S(1)}, f32[8,512]{1,0:T(8,128)S(1)}) custom-call(bf16[256,2048]{1,0:T(8,128)(2,1)} %bitcast.7, f32[1,2048]{1,0:T(1,128)} %bitcast.10, bf16[32,512]{1,0:T(8,128)(2,1)} %wq.1, bf16[32,128]{1,0:T(8,128)(2,1)} %wk.1, bf16[32,128]{1,0:T(8,128)(2,1)} %wv.1, bf16[32,512]{1,0:T(8,128)(2,1)} %wp.1, f32[16]{0:T(128)} %sink_hbm.1, ...), custom_call_target="tpu_custom_call" | custom-call | tf_op jit(solution)/shard_map/mixer/pallas_call | solution.py:546
  71.5 1.0 %leave.1 = (bf16[256,2048]{1,0:T(8,128)(2,1)}, f32[8,512]{1,0:T(8,128)}) custom-call(bf16[256,2048]{1,0:T(8,128)(2,1)S(1)} %get-tuple-element.6.result, f32[8,512]{1,0:T(8,128)S(1)} %get-tuple-element.7.logs), custom_call_target="tpu_custom_call" | custom-call | tf_op jit(solution)/shard_map/leave/pallas_call | solution.py:604
